TPU v7x, 512 devices: a whole 4x4x16 slice. The times are simulated.
512 devices in a mesh: sp: 16 (over z), dp: 32 (over y, x, core).
Axes of the slice: x: 4, y: 4, z: 16, core: 2. Of those that a mesh axis runs over, the one named last changes fastest.
Arguments:
- inputs: bfloat16 [32, 2048, 2048], P('dp', 'sp'), may hold values from -0.75 to 0.75
- queries: bfloat16 [32, 2048, 1024], P('dp', 'sp'), may hold values from -18 to 18
- keys: bfloat16 [32, 2048, 256], P('dp', 'sp'), may hold values from -18 to 18
- values: bfloat16 [32, 2048, 256], P('dp', 'sp'), may hold values from -6 to 6
- out_grad: bfloat16 [32, 2048, 1024], P('dp', 'sp'), may hold values from -144 to 144
- query_gain: float32 [64], replicated, may hold values from 0.4 to 6.5
- key_gain: float32 [64], replicated, may hold values from 0.4 to 6.5
- key_matrix: bfloat16 [2048, 256], P('dp'), may hold values from -0.125 to 0.125
- value_matrix: bfloat16 [2048, 256], P('dp'), may hold values from -0.125 to 0.125
Outputs:
- input_grad: bfloat16 [32, 2048, 2048], P('dp', 'sp')
- query_grad: bfloat16 [32, 2048, 1024], P('dp', 'sp')
- key_weight_grad: float32 [2048, 256], P('dp')
- value_weight_grad: float32 [2048, 256], P('dp')
All inputs are finite; a program needn't handle non-finite values.
Results may differ from a plain program's by a relative error of at most 0.024.
The roundings to bfloat16 on the way count: a program that leaves them out, or rounds other values in their place, can miss the bound.
Values may be sent and summed in bfloat16 or wider, within the bound.
A program may use at most 64 MiB of HBM per device.

v0:
```python
import jax
import jax.numpy as jnp
from jax import lax
from jax.sharding import PartitionSpec as P

QUERY_HEADS = 16
KEY_VALUE_HEADS = 4
HEAD_CHANNELS = 64
GRID = 64


rope_base = 10000.0
norm_eps = 0.5
score_scale = 0.125


def copy_for_each(array, axis):
    copies = jnp.broadcast_to(array, (lax.axis_size(axis), *array.shape))
    return lax.all_to_all(copies, axis, split_axis=0, concat_axis=0, tiled=True)


def joined_along(tiles, dim):
    tiles = jnp.moveaxis(tiles, 0, dim)
    dims = tiles.shape
    return tiles.reshape(*dims[:dim], dims[dim] * dims[dim + 1], *dims[dim + 2 :])


def gathered_copies(array, axis, dim):
    tiles = copy_for_each(array, axis)
    return joined_along(tiles, dim)


def in_blocks(array, dim, size):
    dims = array.shape
    tiles = array.reshape(*dims[:dim], size, dims[dim] // size, *dims[dim + 1 :])
    return jnp.moveaxis(tiles, dim, 0)


def sum_at_owner(array, axis, dim):
    tiles = in_blocks(array, dim, lax.axis_size(axis))
    arrived = lax.all_to_all(tiles, axis, split_axis=0, concat_axis=0, tiled=True)
    return arrived.astype(jnp.float32).sum(axis=0)


def of_everyone(array, axis):
    return copy_for_each(array, axis).astype(jnp.float32).sum(axis=0)


def product(pattern, first_op, second_op):
    return jnp.einsum(pattern, first_op, second_op, preferred_element_type=jnp.float32)


def rotary_tables(token_length):
    position = jnp.arange(token_length, dtype=jnp.int32)
    grid_row = (position // GRID).astype(jnp.float32)
    grid_col = (position % GRID).astype(jnp.float32)
    half_pairs = HEAD_CHANNELS // 4
    inv_freq = rope_base ** (-jnp.arange(half_pairs, dtype=jnp.float32) / half_pairs)
    angles = jnp.concatenate([grid_row[:, None] * inv_freq, grid_col[:, None] * inv_freq], axis=1)
    return (jnp.cos(angles), jnp.sin(angles))


def rotate(vector, cos_tab, sin_tab):
    even_part = vector[..., 0::2]
    odd_part = vector[..., 1::2]
    turned = jnp.stack(
        [even_part * cos_tab - odd_part * sin_tab, even_part * sin_tab + odd_part * cos_tab],
        axis=-1,
    )
    return turned.reshape(vector.shape)


def rotate_back(cotangent, cos_tab, sin_tab):
    even_part = cotangent[..., 0::2]
    odd_part = cotangent[..., 1::2]
    turned = jnp.stack(
        [even_part * cos_tab + odd_part * sin_tab, odd_part * cos_tab - even_part * sin_tab],
        axis=-1,
    )
    return turned.reshape(cotangent.shape)


def inverse_rms(vector):
    return lax.rsqrt(jnp.mean(vector * vector, axis=-1, keepdims=True) + norm_eps)


def norm_back(vector, inv_scale, cotangent, gain_vec):
    weighted = cotangent * gain_vec
    inner_mean = jnp.mean(weighted * vector, axis=-1, keepdims=True)
    return inv_scale * (weighted - vector * inv_scale * inv_scale * inner_mean)


def head_grads(
    query_in, key_input, value_input, grad_in, query_gain, key_gain, cos_tab, sin_tab, block_rows
):
    token_length, groups, per_group, head_dim = query_in.shape
    cos_four = cos_tab[:, None, None, :]
    sin_four = sin_tab[:, None, None, :]
    cos_three = cos_tab[:, None, :]
    sin_three = sin_tab[:, None, :]
    query_f = query_in.astype(jnp.float32)
    query_inv = inverse_rms(query_f)
    query_rot = rotate(query_f * query_inv * query_gain, cos_four, sin_four).astype(jnp.bfloat16)
    key_f = key_input.astype(jnp.float32)
    key_inv = inverse_rms(key_f)
    key_rot = rotate(key_f * key_inv * key_gain, cos_three, sin_three).astype(jnp.bfloat16)
    num_blocks = token_length // block_rows
    query_blocks = query_rot.reshape(num_blocks, block_rows, groups, per_group, head_dim)
    grad_blocks = grad_in.reshape(num_blocks, block_rows, groups, per_group, head_dim)

    def attend_block(carried, pieces):
        key_acc, value_acc = carried
        query_piece, grad_piece = pieces
        scores = product("qgrd,cgd->grqc", query_piece, key_rot) * score_scale
        row_max = jnp.max(scores, axis=-1, keepdims=True)
        shifted = jnp.exp(scores - row_max)
        attn_prob = shifted / jnp.sum(shifted, axis=-1, keepdims=True)
        prob_low = attn_prob.astype(jnp.bfloat16)
        prob_grad = product("qgrd,cgd->grqc", grad_piece, value_input)
        row_dot = jnp.sum(attn_prob * prob_grad, axis=-1, keepdims=True)
        score_grad = (attn_prob * (prob_grad - row_dot) * score_scale).astype(jnp.bfloat16)
        dq_piece = product("grqc,cgd->qgrd", score_grad, key_rot)
        key_acc = key_acc + product("grqc,qgrd->cgd", score_grad, query_piece)
        value_acc = value_acc + product("grqc,qgrd->cgd", prob_low, grad_piece)
        return ((key_acc, value_acc), dq_piece)

    empty_acc = jnp.zeros((token_length, groups, head_dim), jnp.float32)
    (key_rot_grad, value_acc), query_rot_grad = lax.scan(
        attend_block, (empty_acc, empty_acc), (query_blocks, grad_blocks)
    )
    query_rot_grad = query_rot_grad.reshape(token_length, groups, per_group, head_dim)
    query_grad = norm_back(
        query_f, query_inv, rotate_back(query_rot_grad, cos_four, sin_four), query_gain
    ).astype(jnp.bfloat16)
    key_portion = norm_back(
        key_f, key_inv, rotate_back(key_rot_grad, cos_three, sin_three), key_gain
    ).astype(jnp.bfloat16)
    return (query_grad, key_portion, value_acc.astype(jnp.bfloat16))


def on_device(
    inputs, queries, keys, values, out_grad, query_gain, key_gain, key_matrix, value_matrix
):
    sp_count = lax.axis_size("sp")
    token_row_block = inputs.shape[1]
    token_length = token_row_block * sp_count
    local_heads = QUERY_HEADS // sp_count
    portion_heads = min(local_heads, QUERY_HEADS // KEY_VALUE_HEADS)
    kv_here = local_heads // portion_heads
    group_copies = QUERY_HEADS // KEY_VALUE_HEADS // portion_heads
    key_value_width = KEY_VALUE_HEADS * HEAD_CHANNELS
    key_positions = jnp.repeat(
        keys[0].reshape(token_row_block, KEY_VALUE_HEADS, HEAD_CHANNELS), group_copies, axis=1
    ).reshape(token_row_block, key_value_width * group_copies)
    value_positions = jnp.repeat(
        values[0].reshape(token_row_block, KEY_VALUE_HEADS, HEAD_CHANNELS), group_copies, axis=1
    ).reshape(token_row_block, key_value_width * group_copies)
    grad_heads, query_heads, key_heads, value_heads = (
        lax.all_to_all(out_grad[0], "sp", split_axis=1, concat_axis=0, tiled=True),
        lax.all_to_all(queries[0], "sp", split_axis=1, concat_axis=0, tiled=True),
        lax.all_to_all(key_positions, "sp", split_axis=1, concat_axis=0, tiled=True),
        lax.all_to_all(value_positions, "sp", split_axis=1, concat_axis=0, tiled=True),
    )
    cos_tab, sin_tab = rotary_tables(token_length)
    query_part, key_portion, value_portion = head_grads(
        query_heads.reshape(token_length, kv_here, portion_heads, HEAD_CHANNELS),
        key_heads.reshape(token_length, kv_here, HEAD_CHANNELS),
        value_heads.reshape(token_length, kv_here, HEAD_CHANNELS),
        grad_heads.reshape(token_length, kv_here, portion_heads, HEAD_CHANNELS),
        query_gain,
        key_gain,
        cos_tab,
        sin_tab,
        min(512, token_length),
    )
    query_tokens, key_token_rows, value_token_rows = (
        lax.all_to_all(
            query_part.reshape(token_length, local_heads * HEAD_CHANNELS),
            "sp",
            split_axis=0,
            concat_axis=1,
            tiled=True,
        ),
        lax.all_to_all(
            key_portion.reshape(token_length, kv_here * HEAD_CHANNELS),
            "sp",
            split_axis=0,
            concat_axis=1,
            tiled=True,
        ),
        lax.all_to_all(
            value_portion.reshape(token_length, kv_here * HEAD_CHANNELS),
            "sp",
            split_axis=0,
            concat_axis=1,
            tiled=True,
        ),
    )
    key_gradient = (
        key_token_rows.reshape(token_row_block, KEY_VALUE_HEADS, group_copies, HEAD_CHANNELS)
        .astype(jnp.float32)
        .sum(axis=2)
        .astype(jnp.bfloat16)
    )
    value_gradient = (
        value_token_rows.reshape(token_row_block, KEY_VALUE_HEADS, group_copies, HEAD_CHANNELS)
        .astype(jnp.float32)
        .sum(axis=2)
        .astype(jnp.bfloat16)
    )
    projection_gradient = jnp.concatenate(
        [
            key_gradient.reshape(token_row_block, key_value_width),
            value_gradient.reshape(token_row_block, key_value_width),
        ],
        axis=1,
    )
    joined_weight = jnp.concatenate([key_matrix, value_matrix], axis=1)
    input_grad = lax.dot_general(
        projection_gradient,
        gathered_copies(joined_weight, "dp", 0),
        (((1,), (1,)), ((), ())),
        preferred_element_type=jnp.float32,
    ).astype(jnp.bfloat16)
    token_in = inputs[0]
    partial_value = sum_at_owner(
        lax.dot_general(
            token_in,
            projection_gradient,
            (((0,), (0,)), ((), ())),
            preferred_element_type=jnp.float32,
        ).astype(jnp.bfloat16),
        "dp",
        0,
    )
    weight_grad = of_everyone(partial_value.astype(jnp.bfloat16), "sp").astype(jnp.float32)
    return (
        input_grad[None],
        query_tokens[None],
        weight_grad[:, :key_value_width],
        weight_grad[:, key_value_width:],
    )


def solution(mesh):
    return jax.shard_map(
        on_device,
        mesh=mesh,
        in_specs=(
            P("dp", "sp", None),
            P("dp", "sp", None),
            P("dp", "sp", None),
            P("dp", "sp", None),
            P("dp", "sp", None),
            P(),
            P(),
            P("dp", None),
            P("dp", None),
        ),
        out_specs=(P("dp", "sp", None), P("dp", "sp", None), P("dp", None), P("dp", None)),
        check_vma=False,
    )
```

profile of v0, /device:TPU:1, one launch (start us, length us, event | category | flops | bytes accessed | tf_op | source)
XLA Modules:
  0.0 385.0 jit_solution(7380003785234417520)
XLA Ops:
  0.7 1.0 copy.101
  2.4 15.7 %all-to-all-start = ((bf16[128,16,64]{0,2,1:T(8,128)(2,1)}), bf16[128,16,64]{0,2,1:T(8,128)(2,1)S(1)}, u32[]{:S(2)}, u32[]{:S(2)}) async-start(bf16[128,16,64]{0,2,1:T(8,128)(2,1)} %bitcast.1), calls=%async_computation | async-start | bytes 524288 | tf_op jit(solution)/shard_map/all_to_all | solution.py:161
  18.2 1.8 copy.103
  20.0 1.8 copy.107
  22.9 9.0 %all-to-all-done = bf16[128,16,64]{0,2,1:T(8,128)(2,1)S(1)} async-done(((bf16[128,16,64]{0,2,1:T(8,128)(2,1)}), bf16[128,16,64]{0,2,1:T(8,128)(2,1)S(1)}, u32[]{:S(2)}, u32[]{:S(2)}) %all-to-all-start) | async-done | bytes 262176 | tf_op jit(solution)/shard_map/all_to_all | solution.py:161
  31.9 10.4 %all-to-all-start.1 = ((bf16[128,16,64]{0,2,1:T(8,128)(2,1)}), bf16[128,16,64]{0,2,1:T(8,128)(2,1)S(1)}, u32[]{:S(2)}, u32[]{:S(2)}) async-start(bf16[128,16,64]{0,2,1:T(8,128)(2,1)} %bitcast.3), calls=%async_computation.1 | async-start | bytes 524288 | tf_op jit(solution)/shard_map/all_to_all | solution.py:160
  44.5 11.7 %all-to-all-done.1 = bf16[128,16,64]{0,2,1:T(8,128)(2,1)S(1)} async-done(((bf16[128,16,64]{0,2,1:T(8,128)(2,1)}), bf16[128,16,64]{0,2,1:T(8,128)(2,1)S(1)}, u32[]{:S(2)}, u32[]{:S(2)}) %all-to-all-start.1) | async-done | bytes 262176 | tf_op jit(solution)/shard_map/all_to_all | solution.py:160
  56.2 10.4 %all-to-all-start.2 = ((bf16[128,16,64]{0,2,1:T(8,128)(2,1)}), bf16[128,16,64]{0,2,1:T(8,128)(2,1)}, u32[]{:S(2)}, u32[]{:S(2)}) async-start(bf16[128,16,64]{0,2,1:T(8,128)(2,1)} %bitcast.15), calls=%async_computation.2 | async-start | bytes 524288 | tf_op jit(solution)/shard_map/all_to_all | solution.py:159
  67.2 13.1 %all-to-all-done.2 = bf16[128,16,64]{0,2,1:T(8,128)(2,1)} async-done(((bf16[128,16,64]{0,2,1:T(8,128)(2,1)}), bf16[128,16,64]{0,2,1:T(8,128)(2,1)}, u32[]{:S(2)}, u32[]{:S(2)}) %all-to-all-start.2) | async-done | bytes 262176 | tf_op jit(solution)/shard_map/all_to_all | solution.py:159
  81.1 10.3 %all-to-all-start.3 = ((bf16[128,16,64]{0,2,1:T(8,128)(2,1)}), bf16[128,16,64]{0,2,1:T(8,128)(2,1)S(1)}, u32[]{:S(2)}, u32[]{:S(2)}) async-start(bf16[128,16,64]{0,2,1:T(8,128)(2,1)} %bitcast.18), calls=%async_computation.3 | async-start | bytes 524288 | tf_op jit(solution)/shard_map/all_to_all | solution.py:162
  91.5 2.0 fusion.40
  94.2 1.0 fusion.38
  96.5 1.1 copy.108
  98.5 6.7 %all-to-all-done.3 = bf16[128,16,64]{0,2,1:T(8,128)(2,1)S(1)} async-done(((bf16[128,16,64]{0,2,1:T(8,128)(2,1)}), bf16[128,16,64]{0,2,1:T(8,128)(2,1)S(1)}, u32[]{:S(2)}, u32[]{:S(2)}) %all-to-all-start.3) | async-done | bytes 262176 | tf_op jit(solution)/shard_map/all_to_all | solution.py:162
  106.2 71.9 %while.15 = (s32[]{:T(128)}, f32[2048,1,64]{0,2,1:T(8,128)S(1)}, f32[2048,1,64]{0,2,1:T(8,128)}, f32[4,512,1,1,64]{1,0,4,3,2:T(4,128)}, bf16[4,512,1,1,64]{1,4,3...) while((s32[]{:T(128)}, f32[2048,1,64]{0,2,1:T(8,128)S(1)}, ...), condition=%wide.region_6.7_spmd.clone, body=%wide.region_2.6_spmd.clone.sunk | while | flops 693631488 | bytes 77226216 | solution.py:128
  106.2 1.7 multiply_reduce_fusion.6
  107.9 1.9 copy-done.1
  110.7 3.5 fusion.80
  114.2 2.5 fusion.77
  116.7 1.5 fusion.78
  119.1 3.6 dynamic_update_slice.6
  122.8 1.4 fusion.79
  124.2 1.7 multiply_reduce_fusion.6
  125.9 1.9 copy-done.1
  128.7 3.5 fusion.80
  132.2 2.5 fusion.77
  134.6 1.5 fusion.78
  137.1 3.6 dynamic_update_slice.6
  140.7 1.4 fusion.79
  142.1 1.7 multiply_reduce_fusion.6
  143.9 1.9 copy-done.1
  146.6 3.5 fusion.80
  150.1 2.5 fusion.77
  152.6 1.5 fusion.78
  155.1 3.6 dynamic_update_slice.6
  158.7 1.4 fusion.79
  160.1 1.7 multiply_reduce_fusion.6
  161.8 1.9 copy-done.1
  164.6 3.5 fusion.80
  168.1 2.5 fusion.77
  170.6 1.5 fusion.78
  173.1 3.6 dynamic_update_slice.6
  176.7 1.4 fusion.79
  178.4 1.9 add_bitcast_fusion.1
  182.5 10.3 %all-to-all-start.4 = ((bf16[16,128,64]{1,2,0:T(8,128)(2,1)}), bf16[16,128,64]{1,2,0:T(8,128)(2,1)S(1)}, u32[]{:S(2)}, u32[]{:S(2)}) async-start(bf16[16,128,64]{1,2,0:T(8,128)(2,1)} %copy.114), calls=%async_computation.4 | async-start | bytes 524288 | tf_op jit(solution)/shard_map/all_to_all | solution.py:184
  194.4 12.2 %all-to-all-done.4 = bf16[16,128,64]{1,2,0:T(8,128)(2,1)S(1)} async-done(((bf16[16,128,64]{1,2,0:T(8,128)(2,1)}), bf16[16,128,64]{1,2,0:T(8,128)(2,1)S(1)}, u32[]{:S(2)}, u32[]{:S(2)}) %all-to-all-start.4) | async-done | bytes 262176 | tf_op jit(solution)/shard_map/all_to_all | solution.py:184
  206.6 10.3 %all-to-all-start.5 = ((bf16[16,128,64]{1,2,0:T(8,128)(2,1)}), bf16[16,128,64]{1,2,0:T(8,128)(2,1)S(1)}, u32[]{:S(2)}, u32[]{:S(2)}) async-start(bf16[16,128,64]{1,2,0:T(8,128)(2,1)} %copy.117), calls=%async_computation.5 | async-start | bytes 524288 | tf_op jit(solution)/shard_map/all_to_all | solution.py:191
  216.9 1.0 add_bitcast_fusion
  219.1 1.0 multiply_convert_fusion
  220.1 10.6 %all-to-all-done.5 = bf16[16,128,64]{1,2,0:T(8,128)(2,1)S(1)} async-done(((bf16[16,128,64]{1,2,0:T(8,128)(2,1)}), bf16[16,128,64]{1,2,0:T(8,128)(2,1)S(1)}, u32[]{:S(2)}, u32[]{:S(2)}) %all-to-all-start.5) | async-done | bytes 262176 | tf_op jit(solution)/shard_map/all_to_all | solution.py:191
  230.6 10.3 %all-to-all-start.7 = ((bf16[16,128,64]{1,2,0:T(8,128)(2,1)}), bf16[16,128,64]{1,2,0:T(8,128)(2,1)S(1)}, u32[]{:S(2)}, u32[]{:S(2)}) async-start(bf16[16,128,64]{1,2,0:T(8,128)(2,1)} %multiply_convert_fusion), calls=%async_computation.7 | async-start | bytes 524288 | tf_op jit(solution)/shard_map/all_to_all | solution.py:177
  241.8 2.5 copy.123
  244.3 10.4 %all-to-all-done.7 = bf16[16,128,64]{1,2,0:T(8,128)(2,1)S(1)} async-done(((bf16[16,128,64]{1,2,0:T(8,128)(2,1)}), bf16[16,128,64]{1,2,0:T(8,128)(2,1)S(1)}, u32[]{:S(2)}, u32[]{:S(2)}) %all-to-all-start.7) | async-done | bytes 262176 | tf_op jit(solution)/shard_map/all_to_all | solution.py:177
  254.7 12.9 %all-to-all-start.8 = ((bf16[32,64,512]{2,1,0:T(8,128)(2,1)}), bf16[32,64,512]{2,1,0:T(8,128)(2,1)S(1)}, u32[]{:S(2)}, u32[]{:S(2)}) async-start(bf16[32,64,512]{2,1,0:T(8,128)(2,1)} %bitcast.242), calls=%async_computation.8 | async-start | bytes 4194304 | tf_op jit(solution)/shard_map/all_to_all | solution.py:41
  267.7 28.6 %all-to-all-done.8 = bf16[32,64,512]{2,1,0:T(8,128)(2,1)S(1)} async-done(((bf16[32,64,512]{2,1,0:T(8,128)(2,1)}), bf16[32,64,512]{2,1,0:T(8,128)(2,1)S(1)}, u32[]{:S(2)}, u32[]{:S(2)}) %all-to-all-start.8) | async-done | bytes 2097184 | tf_op jit(solution)/shard_map/all_to_all | solution.py:41
  296.2 1.7 broadcast_in_dim.27
  298.2 5.4 %all-to-all-start.6 = ((bf16[32,64,512]{2,1,0:T(8,128)(2,1)}), bf16[32,64,512]{2,1,0:T(8,128)(2,1)S(1)}, u32[]{:S(2)}, u32[]{:S(2)}) async-start(bf16[32,64,512]{2,1,0:T(8,128)(2,1)} %broadcast_in_dim.27), calls=%async_computation.6 | async-start | bytes 4194304 | tf_op jit(solution)/shard_map/all_to_all | solution.py:19
  303.6 1.9 reduce_sum.105
  305.5 26.4 %all-to-all-done.6 = bf16[32,64,512]{2,1,0:T(8,128)(2,1)S(1)} async-done(((bf16[32,64,512]{2,1,0:T(8,128)(2,1)}), bf16[32,64,512]{2,1,0:T(8,128)(2,1)S(1)}, u32[]{:S(2)}, u32[]{:S(2)}) %all-to-all-start.6) | async-done | bytes 2097184 | tf_op jit(solution)/shard_map/all_to_all | solution.py:19
  331.9 1.1 broadcast_in_dim.30
  332.9 5.3 %all-to-all-start.9 = ((bf16[16,64,512]{2,1,0:T(8,128)(2,1)}), bf16[16,64,512]{2,1,0:T(8,128)(2,1)}, u32[]{:S(2)}, u32[]{:S(2)}) async-start(bf16[16,64,512]{2,1,0:T(8,128)(2,1)} %broadcast_in_dim.30), calls=%async_computation.9 | async-start | bytes 2097152 | tf_op jit(solution)/shard_map/all_to_all | solution.py:19
  339.1 1.6 fusion.32
  340.7 42.2 %all-to-all-done.9 = bf16[16,64,512]{2,1,0:T(8,128)(2,1)} async-done(((bf16[16,64,512]{2,1,0:T(8,128)(2,1)}), bf16[16,64,512]{2,1,0:T(8,128)(2,1)}, u32[]{:S(2)}, u32[]{:S(2)}) %all-to-all-start.9) | async-done | bytes 1048608 | tf_op jit(solution)/shard_map/all_to_all | solution.py:19
  382.9 1.4 convert_reduce_fusion
  (141 shorter events, 23.5 us)
Async XLA Ops:
  0.6 240.4 %copy-start = (bf16[1,128,2048]{2,1,0:T(8,128)(2,1)S(1)}, bf16[1,128,2048]{2,1,0:T(8,128)(2,1)}, u32[]{:S(2)}) copy-start(bf16[1,128,2048]{2,1,0:T(8,128)(2,1)} %param.11) | copy-start | bytes 1572868
  0.6 42.2 %copy-start.20 = (f32[64]{0:T(128)S(1)}, f32[64]{0:T(128)}, u32[]{:S(2)}) copy-start(f32[64]{0:T(128)} %param.17) | copy-start | bytes 772
  2.4 29.5 %all-to-all-start = ((bf16[128,16,64]{0,2,1:T(8,128)(2,1)}), bf16[128,16,64]{0,2,1:T(8,128)(2,1)S(1)}, u32[]{:S(2)}, u32[]{:S(2)}) async-start(bf16[128,16,64]{0,2,1:T(8,128)(2,1)} %bitcast.1), calls=%async_computation | async-start | bytes 524288 | tf_op jit(solution)/shard_map/all_to_all | solution.py:161
  22.9 68.6 %copy-start.12 = (f32[2048,1,16]{0,2,1:T(8,128)}, f32[2048,1,16]{0,2,1:T(8,128)S(1)}, u32[]{:S(2)}) copy-start(f32[2048,1,16]{0,2,1:T(8,128)S(1)} %get-tuple-element.168) | copy-start | bytes 393220
  22.9 68.6 %copy-start.13 = (f32[2048,1,16]{0,2,1:T(8,128)}, f32[2048,1,16]{0,2,1:T(8,128)S(1)}, u32[]{:S(2)}) copy-start(f32[2048,1,16]{0,2,1:T(8,128)S(1)} %get-tuple-element.177) | copy-start | bytes 393220
  22.9 71.3 %copy-start.8 = (f32[2048,1,1,16]{0,3,2,1:T(8,128)}, f32[2048,1,1,16]{0,3,2,1:T(8,128)S(1)}, u32[]{:S(2)}) copy-start(f32[2048,1,1,16]{0,3,2,1:T(8,128)S(1)} %get-tuple-element.169) | copy-start | bytes 393220
  22.9 71.3 %copy-start.10 = (f32[2048,1,1,16]{0,3,2,1:T(8,128)}, f32[2048,1,1,16]{0,3,2,1:T(8,128)S(1)}, u32[]{:S(2)}) copy-start(f32[2048,1,1,16]{0,3,2,1:T(8,128)S(1)} %get-tuple-element.176) | copy-start | bytes 393220
  31.9 35.1 %copy-start.6 = (bf16[128,16,64]{0,2,1:T(8,128)(2,1)}, bf16[128,16,64]{0,2,1:T(8,128)(2,1)S(1)}, u32[]{:S(2)}) copy-start(bf16[128,16,64]{0,2,1:T(8,128)(2,1)S(1)} %all-to-all-done) | copy-start | bytes 786436
  31.9 35.2 %copy-start.22 = (f32[64]{0:T(128)S(1)}, f32[64]{0:T(128)}, u32[]{:S(2)}) copy-start(f32[64]{0:T(128)} %param.16) | copy-start | bytes 772
  31.9 24.2 %all-to-all-start.1 = ((bf16[128,16,64]{0,2,1:T(8,128)(2,1)}), bf16[128,16,64]{0,2,1:T(8,128)(2,1)S(1)}, u32[]{:S(2)}, u32[]{:S(2)}) async-start(bf16[128,16,64]{0,2,1:T(8,128)(2,1)} %bitcast.3), calls=%async_computation.1 | async-start | bytes 524288 | tf_op jit(solution)/shard_map/all_to_all | solution.py:160
  56.2 37.6 %copy-start.4 = (bf16[128,16,64]{0,2,1:T(8,128)(2,1)}, bf16[128,16,64]{0,2,1:T(8,128)(2,1)S(1)}, u32[]{:S(2)}) copy-start(bf16[128,16,64]{0,2,1:T(8,128)(2,1)S(1)} %all-to-all-done.1) | copy-start | bytes 786436
  56.2 24.2 %all-to-all-start.2 = ((bf16[128,16,64]{0,2,1:T(8,128)(2,1)}), bf16[128,16,64]{0,2,1:T(8,128)(2,1)}, u32[]{:S(2)}, u32[]{:S(2)}) async-start(bf16[128,16,64]{0,2,1:T(8,128)(2,1)} %bitcast.15), calls=%async_computation.2 | async-start | bytes 524288 | tf_op jit(solution)/shard_map/all_to_all | solution.py:159
  81.1 24.1 %all-to-all-start.3 = ((bf16[128,16,64]{0,2,1:T(8,128)(2,1)}), bf16[128,16,64]{0,2,1:T(8,128)(2,1)S(1)}, u32[]{:S(2)}, u32[]{:S(2)}) async-start(bf16[128,16,64]{0,2,1:T(8,128)(2,1)} %bitcast.18), calls=%async_computation.3 | async-start | bytes 524288 | tf_op jit(solution)/shard_map/all_to_all | solution.py:162
  106.2 4.5 %copy-start.14 = (f32[2048,1,64]{0,2,1:T(8,128)S(1)}, f32[2048,1,64]{0,2,1:T(8,128)}, u32[]{:S(2)}) copy-start(f32[2048,1,64]{0,2,1:T(8,128)} %get-tuple-element.249) | copy-start | bytes 1572868 | tf_op jit(solution)/shard_map/while
  107.9 1.9 copy-start.1
  110.7 3.5 copy-start.2
  114.2 2.5 copy-start.15
  124.1 4.5 %copy-start.14 = (f32[2048,1,64]{0,2,1:T(8,128)S(1)}, f32[2048,1,64]{0,2,1:T(8,128)}, u32[]{:S(2)}) copy-start(f32[2048,1,64]{0,2,1:T(8,128)} %get-tuple-element.249) | copy-start | bytes 1572868 | tf_op jit(solution)/shard_map/while
  125.9 1.9 copy-start.1
  128.6 3.5 copy-start.2
  132.1 2.5 copy-start.15
  142.1 4.5 %copy-start.14 = (f32[2048,1,64]{0,2,1:T(8,128)S(1)}, f32[2048,1,64]{0,2,1:T(8,128)}, u32[]{:S(2)}) copy-start(f32[2048,1,64]{0,2,1:T(8,128)} %get-tuple-element.249) | copy-start | bytes 1572868 | tf_op jit(solution)/shard_map/while
  143.9 1.9 copy-start.1
  146.6 3.5 copy-start.2
  150.1 2.5 copy-start.15
  160.1 4.5 %copy-start.14 = (f32[2048,1,64]{0,2,1:T(8,128)S(1)}, f32[2048,1,64]{0,2,1:T(8,128)}, u32[]{:S(2)}) copy-start(f32[2048,1,64]{0,2,1:T(8,128)} %get-tuple-element.249) | copy-start | bytes 1572868 | tf_op jit(solution)/shard_map/while
  161.8 1.9 copy-start.1
  164.6 3.5 copy-start.2
  168.1 2.5 copy-start.15
  178.1 3.2 copy-start.7
  178.1 3.2 copy-start.21
  178.1 14.7 %copy-start.17 = (f32[4,512,1,1,64]{1,0,4,3,2:T(4,128)S(1)}, f32[4,512,1,1,64]{1,0,4,3,2:T(4,128)}, u32[]{:S(2)}) copy-start(f32[4,512,1,1,64]{1,0,4,3,2:T(4,128)} %get-tuple-element.50) | copy-start | bytes 1572868
  180.3 13.2 %copy-start.16 = (f32[2048,1,64]{0,2,1:T(8,128)S(1)}, f32[2048,1,64]{0,2,1:T(8,128)}, u32[]{:S(2)}) copy-start(f32[2048,1,64]{0,2,1:T(8,128)} %get-tuple-element.49) | copy-start | bytes 1572868
  180.8 36.1 %copy-start.9 = (f32[2048,1,1,16]{0,3,2,1:T(8,128)S(1)}, f32[2048,1,1,16]{0,3,2,1:T(8,128)}, u32[]{:S(2)}) copy-start(f32[2048,1,1,16]{0,3,2,1:T(8,128)} %copy-done.8) | copy-start | bytes 393220
  180.8 36.1 %copy-start.11 = (f32[2048,1,1,16]{0,3,2,1:T(8,128)S(1)}, f32[2048,1,1,16]{0,3,2,1:T(8,128)}, u32[]{:S(2)}) copy-start(f32[2048,1,1,16]{0,3,2,1:T(8,128)} %copy-done.10) | copy-start | bytes 393220
  182.5 24.1 %all-to-all-start.4 = ((bf16[16,128,64]{1,2,0:T(8,128)(2,1)}), bf16[16,128,64]{1,2,0:T(8,128)(2,1)S(1)}, u32[]{:S(2)}, u32[]{:S(2)}) async-start(bf16[16,128,64]{1,2,0:T(8,128)(2,1)} %copy.114), calls=%async_computation.4 | async-start | bytes 524288 | tf_op jit(solution)/shard_map/all_to_all | solution.py:184
  193.2 25.7 %copy-start.5 = (bf16[128,16,64]{0,2,1:T(8,128)(2,1)S(1)}, bf16[128,16,64]{0,2,1:T(8,128)(2,1)}, u32[]{:S(2)}) copy-start(bf16[128,16,64]{0,2,1:T(8,128)(2,1)} %copy-done.4) | copy-start | bytes 786436
  193.2 25.7 %copy-start.23 = (f32[64]{0:T(128)S(1)}, f32[64]{0:T(128)}, u32[]{:S(2)}) copy-start(f32[64]{0:T(128)} %param.16) | copy-start | bytes 772
  206.6 24.1 %all-to-all-start.5 = ((bf16[16,128,64]{1,2,0:T(8,128)(2,1)}), bf16[16,128,64]{1,2,0:T(8,128)(2,1)S(1)}, u32[]{:S(2)}, u32[]{:S(2)}) async-start(bf16[16,128,64]{1,2,0:T(8,128)(2,1)} %copy.117), calls=%async_computation.5 | async-start | bytes 524288 | tf_op jit(solution)/shard_map/all_to_all | solution.py:191
  230.6 24.1 %all-to-all-start.7 = ((bf16[16,128,64]{1,2,0:T(8,128)(2,1)}), bf16[16,128,64]{1,2,0:T(8,128)(2,1)S(1)}, u32[]{:S(2)}, u32[]{:S(2)}) async-start(bf16[16,128,64]{1,2,0:T(8,128)(2,1)} %multiply_convert_fusion), calls=%async_computation.7 | async-start | bytes 524288 | tf_op jit(solution)/shard_map/all_to_all | solution.py:177
  241.8 25.9 %copy-start.18 = (bf16[64,256]{1,0:T(8,128)(2,1)S(1)}, bf16[64,256]{1,0:T(8,128)(2,1)}, u32[]{:S(2)}) copy-start(bf16[64,256]{1,0:T(8,128)(2,1)} %param.19) | copy-start | bytes 98308
  241.8 25.9 %copy-start.19 = (bf16[64,256]{1,0:T(8,128)(2,1)S(1)}, bf16[64,256]{1,0:T(8,128)(2,1)}, u32[]{:S(2)}) copy-start(bf16[64,256]{1,0:T(8,128)(2,1)} %param.18) | copy-start | bytes 98308
  254.7 41.5 %all-to-all-start.8 = ((bf16[32,64,512]{2,1,0:T(8,128)(2,1)}), bf16[32,64,512]{2,1,0:T(8,128)(2,1)S(1)}, u32[]{:S(2)}, u32[]{:S(2)}) async-start(bf16[32,64,512]{2,1,0:T(8,128)(2,1)} %bitcast.242), calls=%async_computation.8 | async-start | bytes 4194304 | tf_op jit(solution)/shard_map/all_to_all | solution.py:41
  296.2 2.0 copy-start.3
  298.2 33.7 %all-to-all-start.6 = ((bf16[32,64,512]{2,1,0:T(8,128)(2,1)}), bf16[32,64,512]{2,1,0:T(8,128)(2,1)S(1)}, u32[]{:S(2)}, u32[]{:S(2)}) async-start(bf16[32,64,512]{2,1,0:T(8,128)(2,1)} %broadcast_in_dim.27), calls=%async_computation.6 | async-start | bytes 4194304 | tf_op jit(solution)/shard_map/all_to_all | solution.py:19
  332.9 50.0 %all-to-all-start.9 = ((bf16[16,64,512]{2,1,0:T(8,128)(2,1)}), bf16[16,64,512]{2,1,0:T(8,128)(2,1)}, u32[]{:S(2)}, u32[]{:S(2)}) async-start(bf16[16,64,512]{2,1,0:T(8,128)(2,1)} %broadcast_in_dim.30), calls=%async_computation.9 | async-start | bytes 2097152 | tf_op jit(solution)/shard_map/all_to_all | solution.py:19
where the time goes:
time: 391 us; the launch traced here: 385 us
  waiting for transfers between devices  171 us (44%)
  starting transfers between devices  101 us (26%)
  local copies, waits for them, and re-layouts  48.1 us (12%)
  matrix products  41.5 us (11%)
  other arithmetic  21.2 us (5%)
    all_to_all x2, waiting for transfers between devices, copy_for_each(): return lax.all_to_all(copies, axis, split_axis=0, concat_axis=0, tiled=True)  68.6 us
    dot_general x20, matrix products, product(): jnp.einsum(pattern, first_op, second_op, preferred_element_type=jnp.float32)  39.2 us
    all_to_all x1, waiting for transfers between devices, sum_at_owner(): lax.all_to_all(tiles, axis, split_axis=0, concat_axis=0, tiled=True)  28.6 us
    all_to_all x1, starting transfers between devices, on_device(): lax.all_to_all(key_positions, 'sp', split_axis=1, concat_axis=0, tiled=True)  15.7 us
    dynamic_update_slice x8, local copies, waits for them, and re-layouts, head_grads(): lax.scan(attend_block, (empty_acc, empty_acc), (query_blocks, grad_blocks))  15.1 us
    all_to_all x1, waiting for transfers between devices, on_device(): lax.all_to_all(out_grad[0], 'sp', split_axis=1, concat_axis=0, tiled=True)  13.1 us
    all_to_all x1, starting transfers between devices, sum_at_owner(): lax.all_to_all(tiles, axis, split_axis=0, concat_axis=0, tiled=True)  12.9 us
    all_to_all x1, waiting for transfers between devices, on_device(): lax.all_to_all(key_portion.reshape(token_length, kv_here * HEAD_CHANNELS)...  12.2 us
  transfers between devices with their start and end apart: 10, of which 10 were waited for; matrix products, arithmetic and copies ran while one was open for 7% of the time, Pallas kernels for 0%

commit v1 on v0

v1 whole, which is shorter than its diff:
```python
import functools

import jax
import jax.numpy as jnp
from jax import lax
from jax.experimental import pallas as pl
from jax.experimental.pallas import tpu as pltpu
from jax.sharding import PartitionSpec as P

GROUPS = 4
PER = 4
DIM = 64
HALF = 32
GRID = 64
ROPE_BASE = 10000.0
EPS = 0.5
SCALE = 0.125
KVW = GROUPS * DIM
F32 = jnp.float32
BF16 = jnp.bfloat16

NN = (((1,), (0,)), ((), ()))
NT = (((1,), (1,)), ((), ()))
TN = (((0,), (0,)), ((), ()))


def dot(a, b, dims=NN):
    return lax.dot_general(a, b, dims, preferred_element_type=F32)


def split_pairs(transposed=False):
    r = lax.broadcasted_iota(jnp.int32, (KVW, KVW), 1 if transposed else 0)
    c = lax.broadcasted_iota(jnp.int32, (KVW, KVW), 0 if transposed else 1)
    i = r % DIM
    src = r - i + jnp.where(i < HALF, 2 * i, 2 * i - (DIM - 1))
    return (c == src).astype(F32).astype(BF16)


def eye(n):
    r = lax.broadcasted_iota(jnp.int32, (n, n), 0)
    c = lax.broadcasted_iota(jnp.int32, (n, n), 1)
    return (r == c).astype(F32).astype(BF16)


def inv_rms(a, b):
    ms = (jnp.sum(a * a, axis=0, keepdims=True) + jnp.sum(b * b, axis=0, keepdims=True)) * (1.0 / DIM)
    return lax.rsqrt(ms + EPS)


def rope_fwd(x, cos, sin, gain):
    a, b = x[:HALF], x[HALF:]
    r = inv_rms(a, b)
    a = a * r * gain[:HALF]
    b = b * r * gain[HALF:]
    return jnp.concatenate([a * cos - b * sin, a * sin + b * cos], axis=0)


def rope_bwd(g, x, cos, sin, gain):
    a, b = g[:HALF], g[HALF:]
    ua = (a * cos + b * sin) * gain[:HALF]
    ub = (b * cos - a * sin) * gain[HALF:]
    qa, qb = x[:HALF], x[HALF:]
    r = inv_rms(qa, qb)
    inner = (jnp.sum(ua * qa, axis=0, keepdims=True) + jnp.sum(ub * qb, axis=0, keepdims=True)) * (1.0 / DIM)
    f = r * r * inner
    return jnp.concatenate([r * (ua - qa * f), r * (ub - qb * f)], axis=0)


def prep_kernel(k_ref, v_ref, cs_ref, gain_ref, kv_ref):
    t = k_ref.shape[0]
    cos, sin = cs_ref[:HALF], cs_ref[HALF:]
    xt = dot(split_pairs(), k_ref[...], NT)
    gain = gain_ref[DIM:]
    rot = jnp.concatenate(
        [rope_fwd(xt[DIM * h : DIM * (h + 1)], cos, sin, gain) for h in range(GROUPS)], axis=0
    ).astype(BF16)
    kv_ref[:t] = dot(eye(t), rot, NT).astype(BF16)
    kv_ref[t:] = v_ref[...]


def attn_kernel(
    q_ref, do_ref, kv_ref, cs_ref, gain_ref, qg_ref, dkv_ref,
    qbd, qbdt, obd, obdt, e_ref, dp_ref, mj, mrun, lsum, dsum, qt, dqt,
):
    t = q_ref.shape[0]
    n = kv_ref.shape[0]
    w = PER * t
    cos, sin = cs_ref[:HALF], cs_ref[HALF:]
    gain = gain_ref[:DIM]
    perm = split_pairs()
    ident = eye(t)
    ident_w = eye(KVW)
    qbd[...] = jnp.zeros_like(qbd)
    obd[...] = jnp.zeros_like(obd)
    for g in range(GROUPS):
        xt = dot(perm, q_ref[:, KVW * g : KVW * (g + 1)], NT)
        qt[g] = xt
        ot = dot(ident_w, do_ref[:, KVW * g : KVW * (g + 1)], NT).astype(BF16)
        for h in range(PER):
            rows = slice(DIM * h, DIM * (h + 1))
            rot = rope_fwd(xt[rows], cos, sin, gain).astype(BF16) * jnp.asarray(SCALE, BF16)
            cols = slice(w * g + t * h, w * g + t * (h + 1))
            qbd[DIM * g : DIM * (g + 1), cols] = rot
            obd[DIM * g : DIM * (g + 1), cols] = ot[rows]
    for i in range(GROUPS * PER):
        cols = slice(t * i, t * (i + 1))
        qbdt[cols, :] = dot(ident, qbd[:, cols], NT).astype(BF16)
        obdt[cols, :] = dot(ident, obd[:, cols], NT).astype(BF16)

    mrun[...] = jnp.full_like(mrun, -jnp.inf)
    lsum[...] = jnp.zeros_like(lsum)
    dsum[...] = jnp.zeros_like(dsum)
    dqt[...] = jnp.zeros_like(dqt)

    def gather_block(j, _):
        kb = kv_ref[j, :t]
        vb = kv_ref[j, t:]
        for g in range(GROUPS):
            cols = slice(w * g, w * (g + 1))
            s = dot(kb, qbd[:, cols])
            dp = dot(vb, obd[:, cols])
            m_old = mrun[:, cols]
            m_new = jnp.maximum(m_old, jnp.max(s, axis=0, keepdims=True))
            e = jnp.exp(s - m_new)
            a = jnp.exp(m_old - m_new)
            mrun[:, cols] = m_new
            mj[j, :, cols] = m_new
            lsum[:, cols] = lsum[:, cols] * a + jnp.sum(e, axis=0, keepdims=True)
            dsum[:, cols] = dsum[:, cols] * a + jnp.sum(e * dp, axis=0, keepdims=True)
            e_ref[j, :, cols] = e
            dp_ref[j, :, cols] = dp
        return 0

    lax.fori_loop(0, n, gather_block, 0)
    lsum[...] = 1.0 / lsum[...]
    dsum[...] = dsum[...] * lsum[...]

    def back_block(j, _):
        kt = dot(ident_w, kv_ref[j, :t], NT).astype(BF16)
        dk = jnp.zeros((t, KVW), F32)
        dv = jnp.zeros((t, KVW), F32)
        for g in range(GROUPS):
            cols = slice(w * g, w * (g + 1))
            c = jnp.exp(mj[j, :, cols] - mrun[:, cols]) * lsum[:, cols]
            p = e_ref[j, :, cols] * c
            ds = (p * (dp_ref[j, :, cols] - dsum[:, cols])).astype(BF16)
            dv += dot(p.astype(BF16), obdt[cols, :])
            dk += dot(ds, qbdt[cols, :])
            dqt[DIM * g : DIM * (g + 1)] += dot(kt[DIM * g : DIM * (g + 1)], ds)
        dkv_ref[j, :t] = dk.astype(BF16)
        dkv_ref[j, t:] = dv.astype(BF16)
        return 0

    lax.fori_loop(0, n, back_block, 0)

    perm_t = split_pairs(True)
    for g in range(GROUPS):
        y = jnp.concatenate(
            [
                rope_bwd(
                    dqt[DIM * g : DIM * (g + 1), t * h : t * (h + 1)] * SCALE,
                    qt[g, DIM * h : DIM * (h + 1)], cos, sin, gain,
                )
                for h in range(PER)
            ],
            axis=0,
        ).astype(BF16)
        y = dot(perm_t, y).astype(BF16)
        qg_ref[:, KVW * g : KVW * (g + 1)] = dot(ident, y, NT).astype(BF16)


def finish_kernel(dkv_ref, k_ref, cs_ref, gain_ref, in_ref, w_ref, ig_ref, wp_ref):
    t = k_ref.shape[0]
    cos, sin = cs_ref[:HALF], cs_ref[HALF:]
    gain = gain_ref[DIM:]
    xt = dot(split_pairs(), k_ref[...], NT)
    gt = dot(eye(KVW), dkv_ref[:t], NT)
    y = jnp.concatenate(
        [
            rope_bwd(gt[DIM * h : DIM * (h + 1)], xt[DIM * h : DIM * (h + 1)], cos, sin, gain)
            for h in range(GROUPS)
        ],
        axis=0,
    ).astype(BF16)
    y = dot(split_pairs(True), y).astype(BF16)
    pg = jnp.concatenate([dot(eye(t), y, NT).astype(BF16), dkv_ref[t:]], axis=1)
    ig_ref[...] = dot(pg, w_ref[...], NT).astype(BF16)
    wp_ref[...] = dot(in_ref[...], pg, TN).astype(BF16)


def tables(t):
    pos = lax.axis_index("sp") * t + jnp.arange(t, dtype=jnp.int32)
    row = (pos // GRID).astype(F32)
    col = (pos % GRID).astype(F32)
    m = DIM // 4
    inv = ROPE_BASE ** (-jnp.arange(m, dtype=F32) / m)
    ang = jnp.concatenate([inv[:, None] * row, inv[:, None] * col], axis=0)
    return jnp.concatenate([jnp.cos(ang), jnp.sin(ang)], axis=0)


def split_gain(g, t):
    g = jnp.concatenate([g[0::2], g[1::2]])
    return jnp.broadcast_to(g[:, None], (DIM, t))


def params():
    return pltpu.CompilerParams(vmem_limit_bytes=60 * 1024 * 1024)


def on_device(inputs, queries, keys, values, out_grad, query_gain, key_gain, key_matrix, value_matrix):
    n = lax.axis_size("sp")
    t = inputs.shape[1]
    s = n * t
    q_all = GROUPS * PER * t
    cs = tables(t)
    gains = jnp.concatenate([split_gain(query_gain, t), split_gain(key_gain, t)], axis=0)
    kv = pl.pallas_call(
        prep_kernel, out_shape=jax.ShapeDtypeStruct((2 * t, KVW), BF16), compiler_params=params()
    )(keys[0], values[0], cs, gains)
    kv_all = lax.all_gather(kv, "sp", axis=0, tiled=False)
    w_all = lax.all_gather(jnp.concatenate([key_matrix, value_matrix], axis=1), "dp", axis=0, tiled=True)
    query_grad, dkv = pl.pallas_call(
        attn_kernel,
        out_shape=(
            jax.ShapeDtypeStruct((t, GROUPS * PER * DIM), BF16),
            jax.ShapeDtypeStruct((n, 2 * t, KVW), BF16),
        ),
        scratch_shapes=[
            pltpu.VMEM((KVW, q_all), BF16),
            pltpu.VMEM((q_all, KVW), BF16),
            pltpu.VMEM((KVW, q_all), BF16),
            pltpu.VMEM((q_all, KVW), BF16),
            pltpu.VMEM((n, t, q_all), F32),
            pltpu.VMEM((n, t, q_all), F32),
            pltpu.VMEM((n, 1, q_all), F32),
            pltpu.VMEM((1, q_all), F32),
            pltpu.VMEM((1, q_all), F32),
            pltpu.VMEM((1, q_all), F32),
            pltpu.VMEM((GROUPS, KVW, t), F32),
            pltpu.VMEM((KVW, PER * t), F32),
        ],
        compiler_params=params(),
    )(queries[0], out_grad[0], kv_all, cs, gains)
    mine = lax.psum_scatter(dkv, "sp", scatter_dimension=0, tiled=False)
    input_grad, w_part = pl.pallas_call(
        finish_kernel,
        out_shape=(
            jax.ShapeDtypeStruct((t, inputs.shape[2]), BF16),
            jax.ShapeDtypeStruct((inputs.shape[2], 2 * KVW), BF16),
        ),
        compiler_params=params(),
    )(mine, keys[0], cs, gains, inputs[0], w_all)
    w_mine = lax.psum_scatter(w_part, "dp", scatter_dimension=0, tiled=True)
    w_grad = lax.psum(w_mine.astype(F32), "sp")
    return input_grad[None], query_grad[None], w_grad[:, :KVW], w_grad[:, KVW:]


def solution(mesh):
    row = P("dp", "sp", None)
    return jax.shard_map(
        on_device,
        mesh=mesh,
        in_specs=(row, row, row, row, row, P(), P(), P("dp", None), P("dp", None)),
        out_specs=(row, row, P("dp", None), P("dp", None)),
        check_vma=False,
    )
```

time: 391 us -> 397 us (1.015)
  the two profiles are of different devices: /device:TPU:1 before, /device:TPU:4 now
where the time goes in v1:
time: 397 us
  waiting for transfers between devices  285 us (72%)
  blocking collectives  58.2 us (15%)
  Pallas kernels  33 us (8%)
  between operations  13.8 us (3%)
  local copies, waits for them, and re-layouts  4.46 us (1%)
    reduce_scatter x1, waiting for transfers between devices, on_device(): w_mine = lax.psum_scatter(w_part, 'dp', scatter_dimension=0, tiled=True)  99.4 us
    reduce_scatter x1, waiting for transfers between devices, on_device(): mine = lax.psum_scatter(dkv, 'sp', scatter_dimension=0, tiled=False)  76.9 us
    all_gather x1, waiting for transfers between devices, on_device(): kv_all = lax.all_gather(kv, 'sp', axis=0, tiled=False)  75.7 us
    psum x1, blocking collectives, on_device(): w_grad = lax.psum(w_mine.astype(F32), 'sp')  58.2 us
    all_gather x1, waiting for transfers between devices, on_device(): lax.all_gather(jnp.concatenate([key_matrix, value_matrix], axis=1), 'dp',...  33 us
    pallas_call x1, Pallas kernels, on_device(): pl.pallas_call(attn_kernel, out_shape=(jax.ShapeDtypeStruct((t, GROUPS *...  25.9 us
  transfers between devices with their start and end apart: 4, of which 4 were waited for; matrix products, arithmetic and copies ran while one was open for 0% of the time, Pallas kernels for 7%

profile of v1, /device:TPU:4, one launch (start us, length us, event | category | flops | bytes accessed | tf_op | source)
XLA Modules:
  0.0 396.9 jit_solution(6641745468764842492)
XLA Ops:
  7.2 0.0 all-gather.6.cloned.1.call-start
  7.2 0.8 slice.18
  8.0 0.8 slice.19
  8.8 0.8 slice.20
  9.5 0.8 slice.21
  10.3 0.1 broadcast_multiply_fusion.1
  10.4 0.1 fusion.1
  10.5 0.6 pad_maximum_fusion.1.cs_ref
  11.1 0.1 fusion.3
  11.2 0.7 broadcast.84.gain_ref
  11.9 2.0 shard_map.120
  13.9 0.0 all-gather.6.cloned.1.call-update
  13.9 0.0 all-gather.4.cloned.1.call-start
  14.0 1.4 pad_maximum_fusion
  15.4 0.0 all-gather.4.cloned.1.call-update
  15.4 0.0 reduce-scatter.3.cloned.1.call-start
  15.4 75.7 %all-gather.6.cloned.1.call-done = bf16[4096,256]{1,0:T(8,128)(2,1)} async-done(((bf16[256,256]{1,0:T(8,128)(2,1)}), bf16[4096,256]{1,0:T(8,128)(2,1)}) %all-gather.6.cloned.1.call-update) | async-done | bytes 2097168 | tf_op jit(solution)/shard_map/all_gather | solution.py:220
  91.1 25.9 %shard_map.121 = (bf16[128,1024]{1,0:T(8,128)(2,1)}, bf16[16,256,256]{2,1,0:T(8,128)(2,1)}) custom-call(bf16[128,1024]{1,0:T(8,128)(2,1)} %bitcast.13, bf16[128,1024]{1,0:T(8,128)(2,1)} %bitcast.14, bf16[16,256,256]{2,1,0:T(8,128)(2,1)} %bitcast.9, f32[64,128]{1,0:T(8,128)} %pad_maximum_fusion.1.cs_ref, f32[128,128]{1,0:T(8,128)} %broadcast.84.gain_ref), custom_call_target="tpu_custom_call" | custom-call | tf_op jit(solution)/shard_map/pallas_call | solution.py:222
  117.0 0.0 reduce-scatter.3.cloned.1.call-update
  117.0 0.0 reduce-scatter.5.cloned.1.call-start
  117.0 33.0 %all-gather.4.cloned.1.call-done.w_ref = bf16[2048,512]{1,0:T(8,128)(2,1)} async-done(((bf16[64,512]{1,0:T(8,128)(2,1)}), bf16[2048,512]{1,0:T(8,128)(2,1)}) %all-gather.4.cloned.1.call-update) | async-done | bytes 2097168 | tf_op jit(solution)/shard_map/all_gather | solution.py:221
  150.1 76.9 %reduce-scatter.3.cloned.1.call-done = bf16[1,256,256]{2,1,0:T(8,128)(2,1)} async-done(((bf16[16,256,256]{2,1,0:T(8,128)(2,1)}), bf16[1,256,256]{2,1,0:T(8,128)(2,1)}) %reduce-scatter.3.cloned.1.call-update) | async-done | bytes 131088 | tf_op jit(solution)/shard_map/reduce_scatter | solution.py:244
  226.9 5.1 %shard_map.122 = (bf16[128,2048]{1,0:T(8,128)(2,1)}, bf16[2048,512]{1,0:T(8,128)(2,1)}) custom-call(bf16[256,256]{1,0:T(8,128)(2,1)} %bitcast.15, bf16[128,256]{1,0:T(8,128)(2,1)} %bitcast.12, f32[64,128]{1,0:T(8,128)} %pad_maximum_fusion.1.cs_ref, f32[128,128]{1,0:T(8,128)} %broadcast.84.gain_ref, bf16[128,2048]{1,0:T(8,128)(2,1)} %bitcast.10, ...), custom_call_target="tpu_custom_call" | custom-call | tf_op jit(solution)/shard_map/pallas_call | solution.py:245
  232.0 0.0 reduce-scatter.5.cloned.1.call-update
  232.1 99.4 %reduce-scatter.5.cloned.1.call-done = bf16[64,512]{1,0:T(8,128)(2,1)} async-done(((bf16[2048,512]{1,0:T(8,128)(2,1)}), bf16[64,512]{1,0:T(8,128)(2,1)}) %reduce-scatter.5.cloned.1.call-update) | async-done | bytes 65552 | tf_op jit(solution)/shard_map/reduce_scatter | solution.py:253
  331.5 58.2 %all-reduce.1 = f32[64,512]{1,0:T(8,128)S(1)} all-reduce(bf16[64,512]{1,0:T(8,128)(2,1)} %reduce-scatter.5.cloned.1.call-done), channel_id=1, replica_groups=mesh['sp'=16,'dp'=32] {'sp'}, use_global_device_ids=true, to_apply=%region_2.3 | all-reduce | flops 32768 | bytes 196608 | tf_op jit(solution)/shard_map/psum | solution.py:254
  389.7 0.7 fusion.5
  (2 shorter events, 0.0 us)
Async XLA Ops:
  7.2 83.9 %all-gather.6.cloned.1.call-start = ((), (), s32[]{:S(2)}) async-start(), calls=%async_computation.5 | async-start | bytes 2228224 | tf_op jit(solution)/shard_map/all_gather | solution.py:220
  13.9 136.2 %all-gather.4.cloned.1.call-start = ((), (), s32[]{:S(2)}) async-start(), calls=%async_computation.3 | async-start | bytes 2162688 | tf_op jit(solution)/shard_map/all_gather | solution.py:221
  15.4 211.6 %reduce-scatter.3.cloned.1.call-start = ((), (), s32[]{:S(2)}) async-start(), calls=%async_computation.2 | async-start | bytes 2228224 | tf_op jit(solution)/shard_map/reduce_scatter | solution.py:244
  117.0 214.5 %reduce-scatter.5.cloned.1.call-start = ((), (), s32[]{:S(2)}) async-start(), calls=%async_computation.4 | async-start | bytes 2162688 | tf_op jit(solution)/shard_map/reduce_scatter | solution.py:253
Sparse Core Ops, SparseCore 0:
  14.0 77.0 all-gather.5
  94.8 55.2 all-gather.3
  152.9 73.9 reduce-scatter.2
  232.2 99.2 reduce-scatter.4

commit v2 on v1

v2 whole, which is shorter than its diff:
```python
import functools

import jax
import jax.numpy as jnp
import numpy as np
from jax import lax
from jax.experimental import pallas as pl
from jax.experimental.pallas import tpu as pltpu
from jax.sharding import PartitionSpec as P

GROUPS = 4
PER = 4
DIM = 64
HALF = 32
GRID = 64
ROPE_BASE = 10000.0
EPS = 0.5
SCALE = 0.125
KVW = GROUPS * DIM
HALFW = 2 * DIM
CHUNKS = 4
F32 = jnp.float32
BF16 = jnp.bfloat16
MESH = pl.DeviceIdType.MESH

NN = (((1,), (0,)), ((), ()))
NT = (((1,), (1,)), ((), ()))


def dot(a, b, dims=NN):
    return lax.dot_general(a, b, dims, preferred_element_type=F32)


def split_source(shape, axis):
    r = lax.broadcasted_iota(jnp.int32, shape, axis)
    i = r % DIM
    return r - i + jnp.where(i < HALF, 2 * i, 2 * i - (DIM - 1))


def split_pairs(transposed=False):
    axis = 1 if transposed else 0
    c = lax.broadcasted_iota(jnp.int32, (KVW, KVW), 1 - axis)
    return (c == split_source((KVW, KVW), axis)).astype(F32).astype(BF16)


def split_gain(gain):
    c = lax.broadcasted_iota(jnp.int32, (DIM, DIM), 1)
    pick = c == split_source((DIM, DIM), 0)
    return jnp.sum(jnp.where(pick, gain, 0.0), axis=1, keepdims=True)


def eye(n):
    r = lax.broadcasted_iota(jnp.int32, (n, n), 0)
    c = lax.broadcasted_iota(jnp.int32, (n, n), 1)
    return (r == c).astype(F32).astype(BF16)


def inv_rms(a, b):
    ms = (jnp.sum(a * a, axis=0, keepdims=True) + jnp.sum(b * b, axis=0, keepdims=True)) * (1.0 / DIM)
    return lax.rsqrt(ms + EPS)


def rope_fwd(x, cos, sin, gain):
    a, b = x[:HALF], x[HALF:]
    r = inv_rms(a, b)
    a = a * r * gain[:HALF]
    b = b * r * gain[HALF:]
    return jnp.concatenate([a * cos - b * sin, a * sin + b * cos], axis=0)


def rope_bwd(g, x, cos, sin, gain):
    a, b = g[:HALF], g[HALF:]
    ua = (a * cos + b * sin) * gain[:HALF]
    ub = (b * cos - a * sin) * gain[HALF:]
    qa, qb = x[:HALF], x[HALF:]
    r = inv_rms(qa, qb)
    inner = (jnp.sum(ua * qa, axis=0, keepdims=True) + jnp.sum(ub * qb, axis=0, keepdims=True)) * (1.0 / DIM)
    f = r * r * inner
    return jnp.concatenate([r * (ua - qa * f), r * (ub - qb * f)], axis=0)


def kernel(
    n, nd,
    x_ref, q_ref, k_ref, v_ref, do_ref, qgain_ref, kgain_ref, km_ref, vm_ref, tab_ref,
    ig_ref, qg_ref, kw_ref, vw_ref,
    cs, kvb, w_all, qbd, qbdt, obd, obdt, e_ref, dp_ref, mj, mrun, lsum, dsum, qt, kt, xt, dqt, acc,
    sbuf, rbuf, wp, pbuf, asend, arecv, zsend, zrecv, zall,
    tab_sem, g_send, g_recv, w_send, w_recv, r_send, r_recv, p_send, p_recv, a_send, a_recv,
    z_send, z_recv, y_send, y_recv,
):
    t = q_ref.shape[0]
    w = PER * t
    h = n // 2
    crow = 2 * t // CHUNKS
    wrow = km_ref.shape[0]
    chips = nd // 2
    me = lax.axis_index("sp")
    dme = lax.axis_index("dp")
    core = dme % 2
    chip = dme // 2
    right = (me + 1) % n
    left = (me + n - 1) % n

    table = pltpu.make_async_copy(tab_ref.at[me], cs, tab_sem)
    table.start()
    barrier = pltpu.get_barrier_semaphore()

    def greet_sp(k, _):
        pl.semaphore_signal(barrier, inc=1, device_id={"sp": (me + k) % n}, device_id_type=MESH)
        return 0

    def greet_dp(k, _):
        pl.semaphore_signal(barrier, inc=1, device_id={"dp": (dme + k) % nd}, device_id_type=MESH)
        return 0

    lax.fori_loop(1, n, greet_sp, 0)
    lax.fori_loop(1, nd, greet_dp, 0)

    perm = split_pairs()
    ident = eye(t)
    ident_w = eye(KVW)
    qgain = split_gain(qgain_ref[...])
    kgain = split_gain(kgain_ref[...])
    kt[...] = dot(perm, k_ref[...], NT)
    w_rows = pl.ds(dme * wrow, wrow)
    w_all[w_rows, :KVW] = km_ref[...]
    w_all[w_rows, KVW:] = vm_ref[...]
    table.wait()
    cos, sin = cs[:HALF], cs[HALF:]
    rot = jnp.concatenate(
        [rope_fwd(kt[DIM * g : DIM * (g + 1)], cos, sin, kgain) for g in range(GROUPS)], axis=0
    ).astype(BF16)
    kvb[0, :t] = dot(ident, rot, NT).astype(BF16)
    kvb[0, t:] = v_ref[...]

    def to_right(s, c):
        part = pl.ds(c * crow, crow)
        return pltpu.make_async_remote_copy(
            src_ref=kvb.at[s - 1, part], dst_ref=kvb.at[s, part],
            send_sem=g_send.at[0, s - 1, c], recv_sem=g_recv.at[0, s - 1, c],
            device_id={"sp": right}, device_id_type=MESH,
        )

    def to_left(s, c):
        part = pl.ds(c * crow, crow)
        return pltpu.make_async_remote_copy(
            src_ref=kvb.at[(n + 1 - s) % n, part], dst_ref=kvb.at[n - s, part],
            send_sem=g_send.at[1, s - 1, c], recv_sem=g_recv.at[1, s - 1, c],
            device_id={"sp": left}, device_id_type=MESH,
        )

    def to_plane(k):
        return pltpu.make_async_remote_copy(
            src_ref=w_all.at[w_rows], dst_ref=w_all.at[w_rows],
            send_sem=w_send.at[k], recv_sem=w_recv.at[k],
            device_id={"dp": (dme + k) % nd}, device_id_type=MESH,
        )

    pl.semaphore_wait(barrier, n - 1 + nd - 1)
    for c in range(CHUNKS):
        to_right(1, c).start()
        to_left(1, c).start()

    def start_w(k, _):
        to_plane(k).start()
        return 0

    lax.fori_loop(1, nd, start_w, 0)

    qbd[...] = jnp.zeros_like(qbd)
    obd[...] = jnp.zeros_like(obd)
    for g in range(GROUPS):
        tr = dot(perm, q_ref[:, KVW * g : KVW * (g + 1)], NT)
        qt[g] = tr
        ot = dot(ident_w, do_ref[:, KVW * g : KVW * (g + 1)], NT).astype(BF16)
        for i in range(PER):
            rows = slice(DIM * i, DIM * (i + 1))
            qr = rope_fwd(tr[rows], cos, sin, qgain).astype(BF16) * jnp.asarray(SCALE, BF16)
            cols = slice(w * g + t * i, w * g + t * (i + 1))
            qbd[DIM * g : DIM * (g + 1), cols] = qr
            obd[DIM * g : DIM * (g + 1), cols] = ot[rows]

    mrun[...] = jnp.full_like(mrun, -jnp.inf)
    lsum[...] = jnp.zeros_like(lsum)
    dsum[...] = jnp.zeros_like(dsum)
    dqt[...] = jnp.zeros_like(dqt)

    def first_pass(slots, step, g):
        cols = slice(w * g, w * (g + 1))
        kb = jnp.concatenate([kvb[r, :t] for r in slots], axis=0)
        vb = jnp.concatenate([kvb[r, t:] for r in slots], axis=0)
        s = dot(kb, qbd[:, cols])
        dp = dot(vb, obd[:, cols])
        m_old = mrun[:, cols]
        m_new = jnp.maximum(m_old, jnp.max(s, axis=0, keepdims=True))
        e = jnp.exp(s - m_new)
        a = jnp.exp(m_old - m_new)
        mrun[:, cols] = m_new
        mj[step, :, cols] = m_new
        lsum[:, cols] = lsum[:, cols] * a + jnp.sum(e, axis=0, keepdims=True)
        dsum[:, cols] = dsum[:, cols] * a + jnp.sum(e * dp, axis=0, keepdims=True)
        for i, r in enumerate(slots):
            e_ref[r, :, cols] = e[t * i : t * (i + 1)]
            dp_ref[r, :, cols] = dp[t * i : t * (i + 1)]

    for g in range(GROUPS):
        first_pass((0,), 0, g)

    for c in range(CHUNKS):
        to_right(1, c).wait_recv()
        if h > 2 or c < 2:
            to_right(2, c).start()
        to_left(1, c).wait_recv()
        if h > 2 or c >= 2:
            to_left(2, c).start()

    def gather_step(s, _):
        for c in range(CHUNKS):
            def receive(copy, s=s, c=c):
                copy(s, c).wait_recv()

            def forward(copy, s=s, c=c):
                copy(s + 1, c).start()

            for copy, whole in ((to_right, c < 2), (to_left, c >= 2)):
                if whole:
                    receive(copy)
                    pl.when(s < h)(functools.partial(forward, copy))
                else:
                    pl.when(s < h)(functools.partial(receive, copy))
                    pl.when(s < h - 1)(functools.partial(forward, copy))
            first_pass((s - 1, n + 1 - s), s - 1, c)
        return 0

    lax.fori_loop(2, h + 1, gather_step, 0)
    for g in range(GROUPS):
        first_pass((h,), h, g)

    for i in range(GROUPS * PER):
        cols = slice(t * i, t * (i + 1))
        qbdt[cols, :] = dot(ident, qbd[:, cols], NT).astype(BF16)
        obdt[cols, :] = dot(ident, obd[:, cols], NT).astype(BF16)
    lsum[...] = 1.0 / lsum[...]
    dsum[...] = dsum[...] * lsum[...]

    def second_pass(slots, step, g, place):
        cols = slice(w * g, w * (g + 1))
        half = slice(HALFW * (g // 2), HALFW * (g // 2 + 1))
        rows = len(slots) * t
        kb = jnp.concatenate([kvb[r, :t] for r in slots], axis=0)
        ktg = dot(ident_w[DIM * g : DIM * (g + 1)], kb, NT).astype(BF16)
        coef = jnp.exp(mj[step, :, cols] - mrun[:, cols]) * lsum[:, cols]
        e = jnp.concatenate([e_ref[r, :, cols] for r in slots], axis=0)
        dp = jnp.concatenate([dp_ref[r, :, cols] for r in slots], axis=0)
        p = e * coef
        ds = (p * (dp - dsum[:, cols])).astype(BF16)
        dv = dot(p.astype(BF16), obdt[cols, half])
        dk = dot(ds, qbdt[cols, half])
        c = 2 * (g // 2)
        if g % 2 == 0:
            acc[place, c, :rows] = dv
            acc[place, c + 1, :rows] = dk
        else:
            acc[place, c, :rows] += dv
            acc[place, c + 1, :rows] += dk
        dqt[DIM * g : DIM * (g + 1)] += dot(ktg, ds)

    def pass_on(d, u, c):
        return pltpu.make_async_remote_copy(
            src_ref=sbuf.at[d, u, c], dst_ref=rbuf.at[d, u, c],
            send_sem=r_send.at[d, u, c], recv_sem=r_recv.at[d, u, c],
            device_id={"sp": left if d else right}, device_id_type=MESH,
        )

    for c in range(CHUNKS):
        rbuf[c % 2, 0, c] = jnp.zeros((t, HALFW), BF16)
    for g in range(GROUPS):
        second_pass((h,), h, g, 0)
        if g % 2 == 1:
            for c in (g - 1, g):
                d = 1 - c % 2
                sbuf[d, 0, c] = acc[0, c, :t].astype(BF16)
                pass_on(d, 0, c).start()
    for g in range(GROUPS):
        second_pass((h + 1, h - 1), h - 1, g, 1)

    def add_and_send(u, c, place):
        for d in range(2):
            def arrived(d=d):
                pass_on(d, u - 1, c).wait_recv()

            if d == 1 - c % 2:
                arrived()
            else:
                pl.when(u > 1)(arrived)
            total = acc[place, c, t * d : t * (d + 1)] + rbuf[d, u - 1, c].astype(F32)
            sbuf[d, u, c] = total.astype(BF16)
            pass_on(d, u, c).start()

    def reduce_step(u, _):
        for c in range(CHUNKS):
            add_and_send(u, c, u % 2)
            second_pass((h + 1 + u, h - 1 - u), h - 1 - u, c, (u + 1) % 2)
        return 0

    lax.fori_loop(1, h - 1, reduce_step, 0)
    last = (h - 1) % 2
    for c in range(CHUNKS):
        add_and_send(h - 1, c, last)
        second_pass((0,), 0, c, 1 - last)

    perm_t = split_pairs(True)
    for g in range(GROUPS):
        y = jnp.concatenate(
            [
                rope_bwd(
                    dqt[DIM * g : DIM * (g + 1), t * i : t * (i + 1)] * SCALE,
                    qt[g, DIM * i : DIM * (i + 1)], cos, sin, qgain,
                )
                for i in range(PER)
            ],
            axis=0,
        ).astype(BF16)
        y = dot(perm_t, y).astype(BF16)
        qg_ref[:, KVW * g : KVW * (g + 1)] = dot(ident, y, NT).astype(BF16)
    width = x_ref.shape[1]
    for i in range(width // HALFW):
        cols = slice(HALFW * i, HALFW * (i + 1))
        xt[cols, :] = dot(eye(HALFW), x_ref[:, cols], NT).astype(BF16)

    whole = []
    for c in range(CHUNKS):
        for d in range(2):
            pass_on(d, h - 1, c).wait_recv()
        whole.append(
            acc[1 - last, c, :t] + rbuf[0, h - 1, c].astype(F32) + rbuf[1, h - 1, c].astype(F32)
        )
    dkt = jnp.transpose(jnp.concatenate([whole[1], whole[3]], axis=1))
    y = jnp.concatenate(
        [
            rope_bwd(dkt[DIM * g : DIM * (g + 1)], kt[DIM * g : DIM * (g + 1)], cos, sin, kgain)
            for g in range(GROUPS)
        ],
        axis=0,
    ).astype(BF16)
    y = dot(perm_t, y).astype(BF16)
    pg = jnp.concatenate(
        [dot(ident, y, NT).astype(BF16), whole[0].astype(BF16), whole[2].astype(BF16)], axis=1
    )

    def to_partner():
        return pltpu.make_async_remote_copy(
            src_ref=wp.at[1 - core], dst_ref=pbuf, send_sem=p_send, recv_sem=p_recv,
            device_id={"dp": dme + 1 - 2 * core}, device_id_type=MESH,
        )

    def to_chip(k):
        return pltpu.make_async_remote_copy(
            src_ref=asend.at[k], dst_ref=arecv.at[k], send_sem=a_send.at[k], recv_sem=a_recv.at[k],
            device_id={"dp": ((chip + k) % chips) * 2 + core}, device_id_type=MESH,
        )

    per_dot = min(8, nd)
    for i in range(nd // per_dot):
        part = dot(xt[wrow * per_dot * i : wrow * per_dot * (i + 1)], pg).astype(BF16)
        for j in range(per_dot):
            o = per_dot * i + j
            wp[o % 2, o // 2] = part[wrow * j : wrow * (j + 1)]
    to_partner().start()

    def wait_w(k, _):
        to_plane(k).wait_recv()
        return 0

    to_partner().wait_recv()

    def send_chip(k, _):
        o = (chip + k) % chips
        asend[k] = (wp[core, o].astype(F32) + pbuf[o].astype(F32)).astype(BF16)
        to_chip(k).start()
        return 0

    lax.fori_loop(1, chips, send_chip, 0)
    lax.fori_loop(1, nd, wait_w, 0)
    for i in range(width // KVW):
        rows = slice(KVW * i, KVW * (i + 1))
        ig_ref[:, rows] = dot(pg, w_all[rows, :], NT).astype(BF16)

    def take_chip(k, total):
        to_chip(k).wait_recv()
        return total + arecv[k].astype(F32)

    mine = wp[core, chip].astype(F32) + pbuf[chip].astype(F32)
    mine = lax.fori_loop(1, chips, take_chip, mine).astype(BF16)

    zrow = zsend.shape[1]
    ncol = 2 * KVW // HALFW
    for i in range(n):
        zsend[i] = mine[zrow * (i // ncol) : zrow * (i // ncol + 1), HALFW * (i % ncol) : HALFW * (i % ncol + 1)]

    def to_depth(k):
        return pltpu.make_async_remote_copy(
            src_ref=zsend.at[(me + k) % n], dst_ref=zrecv.at[k],
            send_sem=z_send.at[k], recv_sem=z_recv.at[k],
            device_id={"sp": (me + k) % n}, device_id_type=MESH,
        )

    def to_all(k):
        return pltpu.make_async_remote_copy(
            src_ref=zall.at[me], dst_ref=zall.at[me],
            send_sem=y_send.at[k], recv_sem=y_recv.at[k],
            device_id={"sp": (me + k) % n}, device_id_type=MESH,
        )

    def start_depth(k, _):
        to_depth(k).start()
        return 0

    def take_depth(k, total):
        to_depth(k).wait_recv()
        return total + zrecv[k].astype(F32)

    def start_all(k, _):
        to_all(k).start()
        return 0

    def wait_all(k, _):
        to_all(k).wait_recv()
        return 0

    lax.fori_loop(1, n, start_depth, 0)
    piece = lax.fori_loop(1, n, take_depth, zsend[me].astype(F32))
    zall[me] = piece.astype(BF16)
    lax.fori_loop(1, n, start_all, 0)
    lax.fori_loop(1, n, wait_all, 0)
    for i in range(n):
        rows = slice(zrow * (i // ncol), zrow * (i // ncol + 1))
        col = i % ncol
        out = kw_ref if col < ncol // 2 else vw_ref
        col = col % (ncol // 2)
        out[rows, HALFW * col : HALFW * (col + 1)] = zall[i].astype(F32)

    def drain_gather(s, _):
        for c in range(CHUNKS):
            to_right(s, c).wait_send()
            to_left(s, c).wait_send()
        return 0

    lax.fori_loop(1, h, drain_gather, 0)
    for c in range(CHUNKS):
        (to_right if c < 2 else to_left)(h, c).wait_send()
        pass_on(1 - c % 2, 0, c).wait_send()

    def drain_reduce(u, _):
        for c in range(CHUNKS):
            pass_on(0, u, c).wait_send()
            pass_on(1, u, c).wait_send()
        return 0

    lax.fori_loop(1, h, drain_reduce, 0)

    def drain_dp(k, _):
        to_plane(k).wait_send()
        return 0

    lax.fori_loop(1, nd, drain_dp, 0)
    to_partner().wait_send()

    def drain_chip(k, _):
        to_chip(k).wait_send()
        return 0

    lax.fori_loop(1, chips, drain_chip, 0)

    def drain_sp(k, _):
        to_depth(k).wait_send()
        to_all(k).wait_send()
        return 0

    lax.fori_loop(1, n, drain_sp, 0)


def tables(n, t):
    pos = np.arange(n * t)
    row = (pos // GRID).astype(np.float32)
    col = (pos % GRID).astype(np.float32)
    m = DIM // 4
    inv = (np.float32(ROPE_BASE) ** (-np.arange(m, dtype=np.float32) / np.float32(m))).astype(np.float32)
    ang = np.concatenate([inv[:, None] * row, inv[:, None] * col], axis=0)
    cs = np.concatenate([np.cos(ang), np.sin(ang)], axis=0).astype(np.float32)
    return np.ascontiguousarray(cs.reshape(2 * HALF, n, t).transpose(1, 0, 2))


def on_device(n, nd, inputs, queries, keys, values, out_grad, query_gain, key_gain, key_matrix, value_matrix):
    t = inputs.shape[1]
    width = inputs.shape[2]
    wrow = key_matrix.shape[0]
    q_all = GROUPS * PER * t
    h = n // 2
    chips = nd // 2
    zrow = wrow * 2 * KVW // HALFW // n
    dma = pltpu.SemaphoreType.DMA
    vmem = pl.BlockSpec(memory_space=pltpu.VMEM)
    shape = jax.ShapeDtypeStruct
    input_grad, query_grad, kw, vw = pl.pallas_call(
        functools.partial(kernel, n, nd),
        out_shape=(
            shape((t, width), BF16),
            shape((t, GROUPS * PER * DIM), BF16),
            shape((wrow, KVW), F32),
            shape((wrow, KVW), F32),
        ),
        in_specs=[vmem] * 9 + [pl.BlockSpec(memory_space=pl.ANY)],
        out_specs=(vmem,) * 4,
        scratch_shapes=[
            pltpu.VMEM((2 * HALF, t), F32),
            pltpu.VMEM((n, 2 * t, KVW), BF16),
            pltpu.VMEM((width, 2 * KVW), BF16),
            pltpu.VMEM((KVW, q_all), BF16),
            pltpu.VMEM((q_all, KVW), BF16),
            pltpu.VMEM((KVW, q_all), BF16),
            pltpu.VMEM((q_all, KVW), BF16),
            pltpu.VMEM((n, t, q_all), F32),
            pltpu.VMEM((n, t, q_all), F32),
            pltpu.VMEM((h + 1, 1, q_all), F32),
            pltpu.VMEM((1, q_all), F32),
            pltpu.VMEM((1, q_all), F32),
            pltpu.VMEM((1, q_all), F32),
            pltpu.VMEM((GROUPS, KVW, t), F32),
            pltpu.VMEM((KVW, t), F32),
            pltpu.VMEM((width, t), BF16),
            pltpu.VMEM((KVW, PER * t), F32),
            pltpu.VMEM((2, CHUNKS, 2 * t, HALFW), F32),
            pltpu.VMEM((2, h, CHUNKS, t, HALFW), BF16),
            pltpu.VMEM((2, h, CHUNKS, t, HALFW), BF16),
            pltpu.VMEM((2, chips, wrow, 2 * KVW), BF16),
            pltpu.VMEM((chips, wrow, 2 * KVW), BF16),
            pltpu.VMEM((chips, wrow, 2 * KVW), BF16),
            pltpu.VMEM((chips, wrow, 2 * KVW), BF16),
            pltpu.VMEM((n, zrow, HALFW), BF16),
            pltpu.VMEM((n, zrow, HALFW), BF16),
            pltpu.VMEM((n, zrow, HALFW), BF16),
            dma,
            dma((2, h, CHUNKS)),
            dma((2, h, CHUNKS)),
            dma((nd,)),
            dma((nd,)),
            dma((2, h, CHUNKS)),
            dma((2, h, CHUNKS)),
            dma,
            dma,
            dma((chips,)),
            dma((chips,)),
            dma((n,)),
            dma((n,)),
            dma((n,)),
            dma((n,)),
        ],
        compiler_params=pltpu.CompilerParams(
            collective_id=0, has_side_effects=True, vmem_limit_bytes=66_000_000
        ),
    )(
        inputs[0], queries[0], keys[0], values[0], out_grad[0],
        query_gain.reshape(1, DIM), key_gain.reshape(1, DIM), key_matrix, value_matrix,
        jnp.asarray(tables(n, t)),
    )
    return input_grad[None], query_grad[None], kw, vw


def solution(mesh):
    row = P("dp", "sp", None)
    return jax.shard_map(
        functools.partial(on_device, mesh.shape["sp"], mesh.shape["dp"]),
        mesh=mesh,
        in_specs=(row, row, row, row, row, P(), P(), P("dp", None), P("dp", None)),
        out_specs=(row, row, P("dp", None), P("dp", None)),
        check_vma=False,
    )
```

time: 397 us -> 120 us (0.30)
  the two profiles are of different devices: /device:TPU:4 before, /device:TPU:1 now
where the time goes in v2:
time: 120 us; the launch traced here: 119 us
  Pallas kernels  114 us (95%)
  local copies, waits for them, and re-layouts  4.28 us (4%)
    pallas_call x1, Pallas kernels, on_device(): pl.pallas_call(functools.partial(kernel, n, nd), out_shape=(shape((t, wid...  114 us
    unnamed x10, local copies, waits for them, and re-layouts  4.28 us

profile of v2, /device:TPU:1, one launch (start us, length us, event | category | flops | bytes accessed | tf_op | source)
XLA Modules:
  0.0 118.6 jit_solution(15602810255223770612)
XLA Ops:
  0.6 113.7 %shard_map.129 = (bf16[128,2048]{1,0:T(8,128)(2,1)}, bf16[128,1024]{1,0:T(8,128)(2,1)}, f32[64,256]{1,0:T(8,128)}, f32[64,256]{1,0:T(8,128)}) custom-call(bf16[128,2048]{1,0:T(8,128)(2,1)} %bitcast.9, bf16[128,1024]{1,0:T(8,128)(2,1)} %bitcast.12, bf16[128,256]{1,0:T(8,128)(2,1)} %bitcast.14, bf16[128,256]{1,0:T(8,128)(2,1)} %bitcast.15, ...), custom_call_target="tpu_custom_call" | custom-call | tf_op jit(solution)/shard_map/pallas_call | solution.py:505
  114.4 0.0 copy-start
  114.4 1.9 %copy.18 = bf16[1,128,2048]{2,1,0:T(8,128)(2,1)} copy(bf16[1,128,2048]{2,1,0:T(8,128)(2,1)} %bitcast.10) | data formatting | bytes 1048576
  116.3 0.0 copy-done
  116.3 0.0 copy-start.2
  116.3 0.7 copy.19
  117.0 0.2 copy-done.2
  117.2 0.0 copy-start.1
  117.2 0.6 copy.20
  117.8 0.2 copy-done.1
  118.0 0.6 copy.21
Async XLA Ops:
  114.4 1.9 %copy-start = (bf16[128,1024]{1,0:T(8,128)(2,1)S(1)}, bf16[128,1024]{1,0:T(8,128)(2,1)}, u32[]{:S(2)}) copy-start(bf16[128,1024]{1,0:T(8,128)(2,1)} %get-tuple-element.9) | copy-start | bytes 786436
  116.3 0.9 copy-start.2
  117.2 0.9 copy-start.1

commit v3 on v2

--- a/solution.py
+++ b/solution.py
@@ -19,6 +19,8 @@
 KVW = GROUPS * DIM
 HALFW = 2 * DIM
 CHUNKS = 4
+PARTS = 4
+SUBS = 1
 F32 = jnp.float32
 BF16 = jnp.bfloat16
 MESH = pl.DeviceIdType.MESH
@@ -81,17 +83,19 @@
 
 def kernel(
     n, nd,
-    x_ref, q_ref, k_ref, v_ref, do_ref, qgain_ref, kgain_ref, km_ref, vm_ref, tab_ref,
-    ig_ref, qg_ref, kw_ref, vw_ref,
+    k_ref, v_ref, qgain_ref, kgain_ref, km_ref, vm_ref, x_hbm, q_hbm, do_hbm, tab_ref,
+    ig_ref, qg_ref, zall,
+    x_ref, q_ref, do_ref,
     cs, kvb, w_all, qbd, qbdt, obd, obdt, e_ref, dp_ref, mj, mrun, lsum, dsum, qt, kt, xt, dqt, acc,
-    sbuf, rbuf, wp, pbuf, asend, arecv, zsend, zrecv, zall,
-    tab_sem, g_send, g_recv, w_send, w_recv, r_send, r_recv, p_send, p_recv, a_send, a_recv,
+    sbuf, rbuf, wp, pbuf, asend, arecv, zsend, zrecv,
+    in_sem, tab_sem, g_send, g_recv, w_send, w_recv, r_send, r_recv, p_send, p_recv, a_send, a_recv,
     z_send, z_recv, y_send, y_recv,
 ):
     t = q_ref.shape[0]
     w = PER * t
     h = n // 2
-    crow = 2 * t // CHUNKS
+    crow = 2 * t // PARTS
+    srow = t // SUBS
     wrow = km_ref.shape[0]
     chips = nd // 2
     me = lax.axis_index("sp")
@@ -101,8 +105,17 @@
     right = (me + 1) % n
     left = (me + n - 1) % n
 
+    def wait_bytes(ref, sem):
+        pltpu.make_async_copy(ref, ref, sem).wait()
+
     table = pltpu.make_async_copy(tab_ref.at[me], cs, tab_sem)
     table.start()
+    fetch_q = pltpu.make_async_copy(q_hbm, q_ref, in_sem.at[0])
+    fetch_do = pltpu.make_async_copy(do_hbm, do_ref, in_sem.at[1])
+    fetch_x = pltpu.make_async_copy(x_hbm, x_ref, in_sem.at[2])
+    fetch_q.start()
+    fetch_do.start()
+    fetch_x.start()
     barrier = pltpu.get_barrier_semaphore()
 
     def greet_sp(k, _):
@@ -137,7 +150,7 @@
         part = pl.ds(c * crow, crow)
         return pltpu.make_async_remote_copy(
             src_ref=kvb.at[s - 1, part], dst_ref=kvb.at[s, part],
-            send_sem=g_send.at[0, s - 1, c], recv_sem=g_recv.at[0, s - 1, c],
+            send_sem=g_send, recv_sem=g_recv.at[0, s - 1, c],
             device_id={"sp": right}, device_id_type=MESH,
         )
 
@@ -145,19 +158,19 @@
         part = pl.ds(c * crow, crow)
         return pltpu.make_async_remote_copy(
             src_ref=kvb.at[(n + 1 - s) % n, part], dst_ref=kvb.at[n - s, part],
-            send_sem=g_send.at[1, s - 1, c], recv_sem=g_recv.at[1, s - 1, c],
+            send_sem=g_send, recv_sem=g_recv.at[1, s - 1, c],
             device_id={"sp": left}, device_id_type=MESH,
         )
 
     def to_plane(k):
         return pltpu.make_async_remote_copy(
             src_ref=w_all.at[w_rows], dst_ref=w_all.at[w_rows],
-            send_sem=w_send.at[k], recv_sem=w_recv.at[k],
+            send_sem=w_send, recv_sem=w_recv,
             device_id={"dp": (dme + k) % nd}, device_id_type=MESH,
         )
 
     pl.semaphore_wait(barrier, n - 1 + nd - 1)
-    for c in range(CHUNKS):
+    for c in range(PARTS):
         to_right(1, c).start()
         to_left(1, c).start()
 
@@ -167,6 +180,8 @@
 
     lax.fori_loop(1, nd, start_w, 0)
 
+    fetch_q.wait()
+    fetch_do.wait()
     qbd[...] = jnp.zeros_like(qbd)
     obd[...] = jnp.zeros_like(obd)
     for g in range(GROUPS):
@@ -205,24 +220,28 @@
 
     for g in range(GROUPS):
         first_pass((0,), 0, g)
-
-    for c in range(CHUNKS):
+    for i in range(GROUPS * PER):
+        cols = slice(t * i, t * (i + 1))
+        qbdt[cols, :] = dot(ident, qbd[:, cols], NT).astype(BF16)
+        obdt[cols, :] = dot(ident, obd[:, cols], NT).astype(BF16)
+
+    for c in range(PARTS):
         to_right(1, c).wait_recv()
-        if h > 2 or c < 2:
+        if h > 2 or c < PARTS // 2:
             to_right(2, c).start()
         to_left(1, c).wait_recv()
-        if h > 2 or c >= 2:
+        if h > 2 or c >= PARTS // 2:
             to_left(2, c).start()
 
     def gather_step(s, _):
-        for c in range(CHUNKS):
+        for c in range(PARTS):
             def receive(copy, s=s, c=c):
                 copy(s, c).wait_recv()
 
             def forward(copy, s=s, c=c):
                 copy(s + 1, c).start()
 
-            for copy, whole in ((to_right, c < 2), (to_left, c >= 2)):
+            for copy, whole in ((to_right, c < PARTS // 2), (to_left, c >= PARTS // 2)):
                 if whole:
                     receive(copy)
                     pl.when(s < h)(functools.partial(forward, copy))
@@ -236,10 +255,6 @@
     for g in range(GROUPS):
         first_pass((h,), h, g)
 
-    for i in range(GROUPS * PER):
-        cols = slice(t * i, t * (i + 1))
-        qbdt[cols, :] = dot(ident, qbd[:, cols], NT).astype(BF16)
-        obdt[cols, :] = dot(ident, obd[:, cols], NT).astype(BF16)
     lsum[...] = 1.0 / lsum[...]
     dsum[...] = dsum[...] * lsum[...]
 
@@ -265,10 +280,11 @@
             acc[place, c + 1, :rows] += dk
         dqt[DIM * g : DIM * (g + 1)] += dot(ktg, ds)
 
-    def pass_on(d, u, c):
-        return pltpu.make_async_remote_copy(
-            src_ref=sbuf.at[d, u, c], dst_ref=rbuf.at[d, u, c],
-            send_sem=r_send.at[d, u, c], recv_sem=r_recv.at[d, u, c],
+    def pass_on(d, u, c, b):
+        part = pl.ds(srow * b, srow)
+        return pltpu.make_async_remote_copy(
+            src_ref=sbuf.at[d, u, c, part], dst_ref=rbuf.at[d, u, c, part],
+            send_sem=r_send, recv_sem=r_recv.at[d, u, c, b],
             device_id={"sp": left if d else right}, device_id_type=MESH,
         )
 
@@ -280,22 +296,25 @@
             for c in (g - 1, g):
                 d = 1 - c % 2
                 sbuf[d, 0, c] = acc[0, c, :t].astype(BF16)
-                pass_on(d, 0, c).start()
+                for b in range(SUBS):
+                    pass_on(d, 0, c, b).start()
     for g in range(GROUPS):
         second_pass((h + 1, h - 1), h - 1, g, 1)
 
     def add_and_send(u, c, place):
-        for d in range(2):
-            def arrived(d=d):
-                pass_on(d, u - 1, c).wait_recv()
-
-            if d == 1 - c % 2:
-                arrived()
-            else:
-                pl.when(u > 1)(arrived)
-            total = acc[place, c, t * d : t * (d + 1)] + rbuf[d, u - 1, c].astype(F32)
-            sbuf[d, u, c] = total.astype(BF16)
-            pass_on(d, u, c).start()
+        for b in range(SUBS):
+            for d in range(2):
+                def arrived(d=d, b=b):
+                    pass_on(d, u - 1, c, b).wait_recv()
+
+                if d == 1 - c % 2:
+                    arrived()
+                else:
+                    pl.when(u > 1)(arrived)
+                part = slice(srow * b, srow * (b + 1))
+                own = acc[place, c, t * d + srow * b : t * d + srow * (b + 1)]
+                sbuf[d, u, c, part] = (own + rbuf[d, u - 1, c, part].astype(F32)).astype(BF16)
+                pass_on(d, u, c, b).start()
 
     def reduce_step(u, _):
         for c in range(CHUNKS):
@@ -323,6 +342,7 @@
         ).astype(BF16)
         y = dot(perm_t, y).astype(BF16)
         qg_ref[:, KVW * g : KVW * (g + 1)] = dot(ident, y, NT).astype(BF16)
+    fetch_x.wait()
     width = x_ref.shape[1]
     for i in range(width // HALFW):
         cols = slice(HALFW * i, HALFW * (i + 1))
@@ -330,8 +350,9 @@
 
     whole = []
     for c in range(CHUNKS):
-        for d in range(2):
-            pass_on(d, h - 1, c).wait_recv()
+        for b in range(SUBS):
+            for d in range(2):
+                pass_on(d, h - 1, c, b).wait_recv()
         whole.append(
             acc[1 - last, c, :t] + rbuf[0, h - 1, c].astype(F32) + rbuf[1, h - 1, c].astype(F32)
         )
@@ -356,7 +377,7 @@
 
     def to_chip(k):
         return pltpu.make_async_remote_copy(
-            src_ref=asend.at[k], dst_ref=arecv.at[k], send_sem=a_send.at[k], recv_sem=a_recv.at[k],
+            src_ref=asend.at[k], dst_ref=arecv.at[k], send_sem=a_send, recv_sem=a_recv.at[k],
             device_id={"dp": ((chip + k) % chips) * 2 + core}, device_id_type=MESH,
         )
 
@@ -368,10 +389,6 @@
             wp[o % 2, o // 2] = part[wrow * j : wrow * (j + 1)]
     to_partner().start()
 
-    def wait_w(k, _):
-        to_plane(k).wait_recv()
-        return 0
-
     to_partner().wait_recv()
 
     def send_chip(k, _):
@@ -381,7 +398,7 @@
         return 0
 
     lax.fori_loop(1, chips, send_chip, 0)
-    lax.fori_loop(1, nd, wait_w, 0)
+    wait_bytes(w_all.at[pl.ds(0, wrow * (nd - 1))], w_recv)
     for i in range(width // KVW):
         rows = slice(KVW * i, KVW * (i + 1))
         ig_ref[:, rows] = dot(pg, w_all[rows, :], NT).astype(BF16)
@@ -401,14 +418,14 @@
     def to_depth(k):
         return pltpu.make_async_remote_copy(
             src_ref=zsend.at[(me + k) % n], dst_ref=zrecv.at[k],
-            send_sem=z_send.at[k], recv_sem=z_recv.at[k],
+            send_sem=z_send, recv_sem=z_recv,
             device_id={"sp": (me + k) % n}, device_id_type=MESH,
         )
 
     def to_all(k):
         return pltpu.make_async_remote_copy(
             src_ref=zall.at[me], dst_ref=zall.at[me],
-            send_sem=y_send.at[k], recv_sem=y_recv.at[k],
+            send_sem=y_send, recv_sem=y_recv,
             device_id={"sp": (me + k) % n}, device_id_type=MESH,
         )
 
@@ -417,67 +434,45 @@
         return 0
 
     def take_depth(k, total):
-        to_depth(k).wait_recv()
         return total + zrecv[k].astype(F32)
 
     def start_all(k, _):
         to_all(k).start()
         return 0
 
-    def wait_all(k, _):
-        to_all(k).wait_recv()
-        return 0
-
     lax.fori_loop(1, n, start_depth, 0)
+    wait_bytes(zrecv.at[pl.ds(0, n - 1)], z_recv)
     piece = lax.fori_loop(1, n, take_depth, zsend[me].astype(F32))
     zall[me] = piece.astype(BF16)
     lax.fori_loop(1, n, start_all, 0)
-    lax.fori_loop(1, n, wait_all, 0)
+    wait_bytes(zall.at[pl.ds(0, n - 1)], y_recv)
+    wait_bytes(kvb.at[pl.ds(0, n - 1)], g_send)
+    wait_bytes(w_all.at[pl.ds(0, wrow * (nd - 1))], w_send)
+    wait_bytes(sbuf.at[0], r_send)
+    wait_bytes(sbuf.at[1, pl.ds(0, h - 1)], r_send)
+    to_partner().wait_send()
+    wait_bytes(asend.at[pl.ds(0, chips - 1)], a_send)
+    wait_bytes(zsend.at[pl.ds(0, n - 1)], z_send)
+    wait_bytes(zall.at[pl.ds(0, n - 1)], y_send)
+
+
+def results(ig, qg, zall, ig_out, qg_out, kw_out, vw_out, kw, vw, sem):
+    copies = [pltpu.make_async_copy(ig, ig_out, sem.at[0]), pltpu.make_async_copy(qg, qg_out, sem.at[1])]
+    for copy in copies:
+        copy.start()
+    n, zrow, _ = zall.shape
+    ncol = 2 * KVW // HALFW
     for i in range(n):
         rows = slice(zrow * (i // ncol), zrow * (i // ncol + 1))
         col = i % ncol
-        out = kw_ref if col < ncol // 2 else vw_ref
+        out = kw if col < ncol // 2 else vw
         col = col % (ncol // 2)
         out[rows, HALFW * col : HALFW * (col + 1)] = zall[i].astype(F32)
-
-    def drain_gather(s, _):
-        for c in range(CHUNKS):
-            to_right(s, c).wait_send()
-            to_left(s, c).wait_send()
-        return 0
-
-    lax.fori_loop(1, h, drain_gather, 0)
-    for c in range(CHUNKS):
-        (to_right if c < 2 else to_left)(h, c).wait_send()
-        pass_on(1 - c % 2, 0, c).wait_send()
-
-    def drain_reduce(u, _):
-        for c in range(CHUNKS):
-            pass_on(0, u, c).wait_send()
-            pass_on(1, u, c).wait_send()
-        return 0
-
-    lax.fori_loop(1, h, drain_reduce, 0)
-
-    def drain_dp(k, _):
-        to_plane(k).wait_send()
-        return 0
-
-    lax.fori_loop(1, nd, drain_dp, 0)
-    to_partner().wait_send()
-
-    def drain_chip(k, _):
-        to_chip(k).wait_send()
-        return 0
-
-    lax.fori_loop(1, chips, drain_chip, 0)
-
-    def drain_sp(k, _):
-        to_depth(k).wait_send()
-        to_all(k).wait_send()
-        return 0
-
-    lax.fori_loop(1, n, drain_sp, 0)
+    copies += [pltpu.make_async_copy(kw, kw_out, sem.at[2]), pltpu.make_async_copy(vw, vw_out, sem.at[3])]
+    for copy in copies[2:]:
+        copy.start()
+    for copy in copies:
+        copy.wait()
 
 
 def tables(n, t):
@@ -502,17 +497,20 @@
     dma = pltpu.SemaphoreType.DMA
     vmem = pl.BlockSpec(memory_space=pltpu.VMEM)
     shape = jax.ShapeDtypeStruct
-    input_grad, query_grad, kw, vw = pl.pallas_call(
+    anywhere = pl.BlockSpec(memory_space=pl.ANY)
+    ig, qg, zall = pl.pallas_call(
         functools.partial(kernel, n, nd),
         out_shape=(
-            shape((t, width), BF16),
-            shape((t, GROUPS * PER * DIM), BF16),
-            shape((wrow, KVW), F32),
-            shape((wrow, KVW), F32),
+            pltpu.VMEM((t, width), BF16),
+            pltpu.VMEM((t, GROUPS * PER * DIM), BF16),
+            pltpu.VMEM((n, zrow, HALFW), BF16),
         ),
-        in_specs=[vmem] * 9 + [pl.BlockSpec(memory_space=pl.ANY)],
-        out_specs=(vmem,) * 4,
+        in_specs=[vmem] * 6 + [anywhere] * 4,
+        out_specs=(vmem,) * 3,
         scratch_shapes=[
+            pltpu.VMEM((t, width), BF16),
+            pltpu.VMEM((t, GROUPS * PER * DIM), BF16),
+            pltpu.VMEM((t, GROUPS * PER * DIM), BF16),
             pltpu.VMEM((2 * HALF, t), F32),
             pltpu.VMEM((n, 2 * t, KVW), BF16),
             pltpu.VMEM((width, 2 * KVW), BF16),
@@ -539,31 +537,43 @@
             pltpu.VMEM((chips, wrow, 2 * KVW), BF16),
             pltpu.VMEM((n, zrow, HALFW), BF16),
             pltpu.VMEM((n, zrow, HALFW), BF16),
-            pltpu.VMEM((n, zrow, HALFW), BF16),
-            dma,
-            dma((2, h, CHUNKS)),
-            dma((2, h, CHUNKS)),
-            dma((nd,)),
-            dma((nd,)),
-            dma((2, h, CHUNKS)),
-            dma((2, h, CHUNKS)),
+            dma((3,)),
+            dma,
+            dma,
+            dma((2, h, PARTS)),
+            dma,
+            dma,
+            dma,
+            dma((2, h, CHUNKS, SUBS)),
+            dma,
             dma,
             dma,
             dma((chips,)),
-            dma((chips,)),
-            dma((n,)),
-            dma((n,)),
-            dma((n,)),
-            dma((n,)),
+            dma,
+            dma,
+            dma,
+            dma,
         ],
         compiler_params=pltpu.CompilerParams(
-            collective_id=0, has_side_effects=True, vmem_limit_bytes=66_000_000
+            collective_id=0, has_side_effects=True, vmem_limit_bytes=61_000_000
         ),
     )(
-        inputs[0], queries[0], keys[0], values[0], out_grad[0],
-        query_gain.reshape(1, DIM), key_gain.reshape(1, DIM), key_matrix, value_matrix,
-        jnp.asarray(tables(n, t)),
+        keys[0], values[0], query_gain.reshape(1, DIM), key_gain.reshape(1, DIM), key_matrix, value_matrix,
+        inputs[0], queries[0], out_grad[0], jnp.asarray(tables(n, t)),
     )
+    input_grad, query_grad, kw, vw = pl.pallas_call(
+        results,
+        out_shape=(
+            shape((t, width), BF16),
+            shape((t, GROUPS * PER * DIM), BF16),
+            shape((wrow, KVW), F32),
+            shape((wrow, KVW), F32),
+        ),
+        in_specs=[vmem] * 3,
+        out_specs=(anywhere,) * 4,
+        scratch_shapes=[pltpu.VMEM((wrow, KVW), F32), pltpu.VMEM((wrow, KVW), F32), dma((4,))],
+        compiler_params=pltpu.CompilerParams(vmem_limit_bytes=4 * 1024 * 1024),
+    )(ig, qg, zall)
     return input_grad[None], query_grad[None], kw, vw
 
 

time: 120 us -> 111 us (0.925)
  local copies, waits for them, and re-layouts: 4.28 us -> 0 us
  Pallas kernels: 114 us -> 110 us
    unnamed x10 -> x0, local copies, waits for them, and re-layouts: 4.28 us -> none
    pallas_call x1 -> x2, Pallas kernels: 114 us -> 110 us  [the longest x1 109 us: on_device(): pl.pallas_call(functools.partial(kernel, n, nd), out_shape=(pltpu.VMEM((t...]
where the time goes in v3:
time: 111 us
  Pallas kernels  110 us (99%)
    pallas_call x1, Pallas kernels, on_device(): pl.pallas_call(functools.partial(kernel, n, nd), out_shape=(pltpu.VMEM((t...  109 us

profile of v3, /device:TPU:1, one launch (start us, length us, event | category | flops | bytes accessed | tf_op | source)
XLA Modules:
  0.0 110.7 jit_solution(11496759898954689878)
XLA Ops:
  0.6 109.1 %shard_map.129 = (bf16[128,2048]{1,0:T(8,128)(2,1)S(1)}, bf16[128,1024]{1,0:T(8,128)(2,1)S(1)}, bf16[16,16,128]{2,1,0:T(8,128)(2,1)S(1)}) custom-call(bf16[128,256]{1,0:T(8,128)(2,1)} %bitcast.12, bf16[128,256]{1,0:T(8,128)(2,1)} %bitcast.13, f32[1,64]{1,0:T(1,128)} %bitcast.14, f32[1,64]{1,0:T(1,128)} %bitcast.15, bf16[64,256]{1,0:T(8,128)(2,1)} %km_ref.1, ...), custom_call_target="tpu_custom_call" | custom-call | tf_op jit(solution)/shard_map/pallas_call | solution.py:501
  109.7 0.9 shard_map.130

commit v4 on v3

--- a/solution.py
+++ b/solution.py
@@ -85,10 +85,10 @@
     n, nd,
     k_ref, v_ref, qgain_ref, kgain_ref, km_ref, vm_ref, x_hbm, q_hbm, do_hbm, tab_ref,
     ig_ref, qg_ref, zall,
-    x_ref, q_ref, do_ref,
+    x_ref, q_ref, do_ref, kx, own, ig_s, qg_s,
     cs, kvb, w_all, qbd, qbdt, obd, obdt, e_ref, dp_ref, mj, mrun, lsum, dsum, qt, kt, xt, dqt, acc,
     sbuf, rbuf, wp, pbuf, asend, arecv, zsend, zrecv,
-    in_sem, tab_sem, g_send, g_recv, w_send, w_recv, r_send, r_recv, p_send, p_recv, a_send, a_recv,
+    in_sem, swap_send, back_recv, tab_sem, g_send, g_recv, w_send, w_recv, r_send, r_recv, p_send, p_recv, a_send, a_recv,
     z_send, z_recv, y_send, y_recv,
 ):
     t = q_ref.shape[0]
@@ -104,6 +104,10 @@
     chip = dme // 2
     right = (me + 1) % n
     left = (me + n - 1) % n
+    mate = dme + 1 - 2 * core
+    odd = me % 2 == 1
+    even = me % 2 == 0
+    first_dp = dme + (1 - me % 2) * (1 - 2 * core)
 
     def wait_bytes(ref, sem):
         pltpu.make_async_copy(ref, ref, sem).wait()
@@ -113,9 +117,28 @@
     fetch_q = pltpu.make_async_copy(q_hbm, q_ref, in_sem.at[0])
     fetch_do = pltpu.make_async_copy(do_hbm, do_ref, in_sem.at[1])
     fetch_x = pltpu.make_async_copy(x_hbm, x_ref, in_sem.at[2])
-    fetch_q.start()
-    fetch_do.start()
-    fetch_x.start()
+
+    @pl.when(even)
+    def _():
+        fetch_q.start()
+        fetch_do.start()
+        fetch_x.start()
+
+    def to_mate(i, src, dst, recv_sem):
+        return pltpu.make_async_remote_copy(
+            src_ref=src, dst_ref=dst, send_sem=swap_send.at[i], recv_sem=recv_sem,
+            device_id={"dp": mate}, device_id_type=MESH,
+        )
+
+    swap_kv = to_mate(0, own, kvb.at[0], in_sem.at[3])
+    swaps = [
+        swap_kv,
+        to_mate(1, q_hbm, q_ref, in_sem.at[0]),
+        to_mate(2, do_hbm, do_ref, in_sem.at[1]),
+        to_mate(3, k_ref, kx, in_sem.at[4]),
+        to_mate(4, x_hbm, x_ref, in_sem.at[2]),
+    ]
+    backs = [to_mate(5, qg_s, qg_ref, back_recv.at[0]), to_mate(6, ig_s, ig_ref, back_recv.at[1])]
     barrier = pltpu.get_barrier_semaphore()
 
     def greet_sp(k, _):
@@ -128,6 +151,8 @@
 
     lax.fori_loop(1, n, greet_sp, 0)
     lax.fori_loop(1, nd, greet_dp, 0)
+    for side in (left, right):
+        pl.semaphore_signal(barrier, inc=1, device_id={"sp": side, "dp": mate}, device_id_type=MESH)
 
     perm = split_pairs()
     ident = eye(t)
@@ -143,15 +168,19 @@
     rot = jnp.concatenate(
         [rope_fwd(kt[DIM * g : DIM * (g + 1)], cos, sin, kgain) for g in range(GROUPS)], axis=0
     ).astype(BF16)
-    kvb[0, :t] = dot(ident, rot, NT).astype(BF16)
-    kvb[0, t:] = v_ref[...]
+    own[:t] = dot(ident, rot, NT).astype(BF16)
+    own[t:] = v_ref[...]
+
+    @pl.when(even)
+    def _():
+        kvb[0] = own[...]
 
     def to_right(s, c):
         part = pl.ds(c * crow, crow)
         return pltpu.make_async_remote_copy(
             src_ref=kvb.at[s - 1, part], dst_ref=kvb.at[s, part],
             send_sem=g_send, recv_sem=g_recv.at[0, s - 1, c],
-            device_id={"sp": right}, device_id_type=MESH,
+            device_id={"sp": right, "dp": mate}, device_id_type=MESH,
         )
 
     def to_left(s, c):
@@ -159,7 +188,15 @@
         return pltpu.make_async_remote_copy(
             src_ref=kvb.at[(n + 1 - s) % n, part], dst_ref=kvb.at[n - s, part],
             send_sem=g_send, recv_sem=g_recv.at[1, s - 1, c],
-            device_id={"sp": left}, device_id_type=MESH,
+            device_id={"sp": left, "dp": mate}, device_id_type=MESH,
+        )
+
+    def first_hop(c, d):
+        part = pl.ds(c * crow, crow)
+        return pltpu.make_async_remote_copy(
+            src_ref=own.at[part], dst_ref=kvb.at[n - 1 if d else 1, part],
+            send_sem=g_send, recv_sem=g_recv.at[d, 0, c],
+            device_id={"sp": left if d else right, "dp": first_dp}, device_id_type=MESH,
         )
 
     def to_plane(k):
@@ -169,10 +206,16 @@
             device_id={"dp": (dme + k) % nd}, device_id_type=MESH,
         )
 
-    pl.semaphore_wait(barrier, n - 1 + nd - 1)
+    pl.semaphore_wait(barrier, n - 1 + nd - 1 + 2)
     for c in range(PARTS):
-        to_right(1, c).start()
-        to_left(1, c).start()
+        first_hop(c, 0).start()
+        first_hop(c, 1).start()
+
+    @pl.when(odd)
+    def _():
+        for copy in swaps:
+            copy.start()
+
 
     def start_w(k, _):
         to_plane(k).start()
@@ -218,6 +261,7 @@
             e_ref[r, :, cols] = e[t * i : t * (i + 1)]
             dp_ref[r, :, cols] = dp[t * i : t * (i + 1)]
 
+    pl.when(odd)(swap_kv.wait_recv)
     for g in range(GROUPS):
         first_pass((0,), 0, g)
     for i in range(GROUPS * PER):
@@ -285,7 +329,7 @@
         return pltpu.make_async_remote_copy(
             src_ref=sbuf.at[d, u, c, part], dst_ref=rbuf.at[d, u, c, part],
             send_sem=r_send, recv_sem=r_recv.at[d, u, c, b],
-            device_id={"sp": left if d else right}, device_id_type=MESH,
+            device_id={"sp": left if d else right, "dp": mate}, device_id_type=MESH,
         )
 
     for c in range(CHUNKS):
@@ -341,8 +385,15 @@
             axis=0,
         ).astype(BF16)
         y = dot(perm_t, y).astype(BF16)
-        qg_ref[:, KVW * g : KVW * (g + 1)] = dot(ident, y, NT).astype(BF16)
+        qg_s[:, KVW * g : KVW * (g + 1)] = dot(ident, y, NT).astype(BF16)
+    pl.when(odd)(backs[0].start)
     fetch_x.wait()
+
+    @pl.when(odd)
+    def _():
+        swaps[3].wait_recv()
+        kt[...] = dot(perm, kx[...], NT)
+
     width = x_ref.shape[1]
     for i in range(width // HALFW):
         cols = slice(HALFW * i, HALFW * (i + 1))
@@ -401,7 +452,14 @@
     wait_bytes(w_all.at[pl.ds(0, wrow * (nd - 1))], w_recv)
     for i in range(width // KVW):
         rows = slice(KVW * i, KVW * (i + 1))
-        ig_ref[:, rows] = dot(pg, w_all[rows, :], NT).astype(BF16)
+        ig_s[:, rows] = dot(pg, w_all[rows, :], NT).astype(BF16)
+    pl.when(odd)(backs[1].start)
+
+    @pl.when(even)
+    def _():
+        qg_ref[...] = qg_s[...]
+        ig_ref[...] = ig_s[...]
+
 
     def take_chip(k, total):
         to_chip(k).wait_recv()
@@ -446,6 +504,13 @@
     zall[me] = piece.astype(BF16)
     lax.fori_loop(1, n, start_all, 0)
     wait_bytes(zall.at[pl.ds(0, n - 1)], y_recv)
+    @pl.when(odd)
+    def _():
+        for copy in backs:
+            copy.wait_recv()
+        for copy in swaps + backs:
+            copy.wait_send()
+
     wait_bytes(kvb.at[pl.ds(0, n - 1)], g_send)
     wait_bytes(w_all.at[pl.ds(0, wrow * (nd - 1))], w_send)
     wait_bytes(sbuf.at[0], r_send)
@@ -510,6 +575,10 @@
         scratch_shapes=[
             pltpu.VMEM((t, width), BF16),
             pltpu.VMEM((t, GROUPS * PER * DIM), BF16),
+            pltpu.VMEM((t, GROUPS * PER * DIM), BF16),
+            pltpu.VMEM((t, KVW), BF16),
+            pltpu.VMEM((2 * t, KVW), BF16),
+            pltpu.VMEM((t, width), BF16),
             pltpu.VMEM((t, GROUPS * PER * DIM), BF16),
             pltpu.VMEM((2 * HALF, t), F32),
             pltpu.VMEM((n, 2 * t, KVW), BF16),
@@ -537,7 +606,9 @@
             pltpu.VMEM((chips, wrow, 2 * KVW), BF16),
             pltpu.VMEM((n, zrow, HALFW), BF16),
             pltpu.VMEM((n, zrow, HALFW), BF16),
-            dma((3,)),
+            dma((5,)),
+            dma((7,)),
+            dma((2,)),
             dma,
             dma,
             dma((2, h, PARTS)),

time: 111 us -> 113 us (1.018); the launches traced: 111 us -> 111 us
  no operation moved by 1% of the time
where the time goes in v4:
time: 113 us; the launch traced here: 111 us
  Pallas kernels  110 us (97%)
    pallas_call x1, Pallas kernels, on_device(): pl.pallas_call(functools.partial(kernel, n, nd), out_shape=(pltpu.VMEM((t...  109 us

profile of v4, /device:TPU:1, one launch (start us, length us, event | category | flops | bytes accessed | tf_op | source)
XLA Modules:
  0.0 110.9 jit_solution(17800789964900790675)
XLA Ops:
  0.6 109.3 %shard_map.129 = (bf16[128,2048]{1,0:T(8,128)(2,1)S(1)}, bf16[128,1024]{1,0:T(8,128)(2,1)S(1)}, bf16[16,16,128]{2,1,0:T(8,128)(2,1)S(1)}) custom-call(bf16[128,256]{1,0:T(8,128)(2,1)} %bitcast.12, bf16[128,256]{1,0:T(8,128)(2,1)} %bitcast.13, f32[1,64]{1,0:T(1,128)} %bitcast.14, f32[1,64]{1,0:T(1,128)} %bitcast.15, bf16[64,256]{1,0:T(8,128)(2,1)} %km_ref.1, ...), custom_call_target="tpu_custom_call" | custom-call | tf_op jit(solution)/shard_map/pallas_call | solution.py:566
  109.9 0.9 shard_map.130

commit v5 on v4

--- a/solution.py
+++ b/solution.py
@@ -83,13 +83,13 @@
 
 def kernel(
     n, nd,
-    k_ref, v_ref, qgain_ref, kgain_ref, km_ref, vm_ref, x_hbm, q_hbm, do_hbm, tab_ref,
+    k_hbm, v_hbm, qgain_ref, kgain_ref, km_hbm, vm_hbm, x_hbm, q_hbm, do_hbm, tab_ref,
     ig_ref, qg_ref, zall,
-    x_ref, q_ref, do_ref, kx, own, ig_s, qg_s,
+    k_ref, v_ref, km_ref, vm_ref, xx, q_ref, do_ref, kx, own, ig_s, qg_s,
     cs, kvb, w_all, qbd, qbdt, obd, obdt, e_ref, dp_ref, mj, mrun, lsum, dsum, qt, kt, xt, dqt, acc,
-    sbuf, rbuf, wp, pbuf, asend, arecv, zsend, zrecv,
-    in_sem, swap_send, back_recv, tab_sem, g_send, g_recv, w_send, w_recv, r_send, r_recv, p_send, p_recv, a_send, a_recv,
-    z_send, z_recv, y_send, y_recv,
+    sbuf, rbuf, pgb, asend, arecv, zsend, zrecv,
+    first_sem, in_sem, swap_send, back_recv, tab_sem, g_send, g_recv, w_send, w_recv, r_send, r_recv, a_send, a_recv,
+    z_send, z_recv, y_send, y_recv, plane,
 ):
     t = q_ref.shape[0]
     w = PER * t
@@ -114,15 +114,24 @@
 
     table = pltpu.make_async_copy(tab_ref.at[me], cs, tab_sem)
     table.start()
+    firsts = [
+        pltpu.make_async_copy(src, dst, first_sem.at[i])
+        for i, (src, dst) in enumerate(
+            ((k_hbm, k_ref), (v_hbm, v_ref), (km_hbm, km_ref), (vm_hbm, vm_ref))
+        )
+    ]
+    for copy in firsts:
+        copy.start()
     fetch_q = pltpu.make_async_copy(q_hbm, q_ref, in_sem.at[0])
     fetch_do = pltpu.make_async_copy(do_hbm, do_ref, in_sem.at[1])
-    fetch_x = pltpu.make_async_copy(x_hbm, x_ref, in_sem.at[2])
+    fetch_x = pltpu.make_async_copy(x_hbm, xx.at[0], in_sem.at[2])
 
     @pl.when(even)
     def _():
         fetch_q.start()
         fetch_do.start()
-        fetch_x.start()
+
+    fetch_x.start()
 
     def to_mate(i, src, dst, recv_sem):
         return pltpu.make_async_remote_copy(
@@ -136,29 +145,36 @@
         to_mate(1, q_hbm, q_ref, in_sem.at[0]),
         to_mate(2, do_hbm, do_ref, in_sem.at[1]),
         to_mate(3, k_ref, kx, in_sem.at[4]),
-        to_mate(4, x_hbm, x_ref, in_sem.at[2]),
     ]
+    swap_x = to_mate(4, x_hbm, xx.at[1], in_sem.at[5])
+    swap_pg = to_mate(7, pgb.at[pl.ds(0, t)], pgb.at[pl.ds(t, t)], in_sem.at[6])
     backs = [to_mate(5, qg_s, qg_ref, back_recv.at[0]), to_mate(6, ig_s, ig_ref, back_recv.at[1])]
     barrier = pltpu.get_barrier_semaphore()
 
-    def greet_sp(k, _):
-        pl.semaphore_signal(barrier, inc=1, device_id={"sp": (me + k) % n}, device_id_type=MESH)
-        return 0
-
-    def greet_dp(k, _):
-        pl.semaphore_signal(barrier, inc=1, device_id={"dp": (dme + k) % nd}, device_id_type=MESH)
-        return 0
-
-    lax.fori_loop(1, n, greet_sp, 0)
-    lax.fori_loop(1, nd, greet_dp, 0)
+    xs = 4 if chips == 16 else 2
+    ys = chips // xs
+    row, col = chip // xs, chip % xs
+    beside = [(row * xs + (col + i) % xs) * 2 for i in range(1, xs)]
+    above = [((row + i) % ys * xs + col) * 2 for i in range(1, ys)]
+
+    def greet(where):
+        pl.semaphore_signal(barrier, inc=1, device_id=where, device_id_type=MESH)
+
     for side in (left, right):
-        pl.semaphore_signal(barrier, inc=1, device_id={"sp": side, "dp": mate}, device_id_type=MESH)
+        greet({"sp": side, "dp": dme})
+        greet({"sp": side, "dp": mate})
+    greet({"dp": mate})
+    for other in beside + above:
+        for i in range(2):
+            greet({"dp": other + i})
 
     perm = split_pairs()
     ident = eye(t)
     ident_w = eye(KVW)
     qgain = split_gain(qgain_ref[...])
     kgain = split_gain(kgain_ref[...])
+    for copy in firsts:
+        copy.wait()
     kt[...] = dot(perm, k_ref[...], NT)
     w_rows = pl.ds(dme * wrow, wrow)
     w_all[w_rows, :KVW] = km_ref[...]
@@ -206,7 +222,10 @@
             device_id={"dp": (dme + k) % nd}, device_id_type=MESH,
         )
 
-    pl.semaphore_wait(barrier, n - 1 + nd - 1 + 2)
+    pl.semaphore_wait(barrier, 5 + 2 * len(beside + above))
+    for other in beside:
+        for i in range(2):
+            pl.semaphore_signal(plane, inc=1, device_id={"dp": other + i}, device_id_type=MESH)
     for c in range(PARTS):
         first_hop(c, 0).start()
         first_hop(c, 1).start()
@@ -216,12 +235,12 @@
         for copy in swaps:
             copy.start()
 
+    swap_x.start()
+
 
     def start_w(k, _):
         to_plane(k).start()
         return 0
-
-    lax.fori_loop(1, nd, start_w, 0)
 
     fetch_q.wait()
     fetch_do.wait()
@@ -278,6 +297,11 @@
             to_left(2, c).start()
 
     def gather_step(s, _):
+        @pl.when(s == min(3, h))
+        def _():
+            pl.semaphore_wait(plane, 2 * len(beside))
+            lax.fori_loop(1, nd, start_w, 0)
+
         for c in range(PARTS):
             def receive(copy, s=s, c=c):
                 copy(s, c).wait_recv()
@@ -386,18 +410,25 @@
         ).astype(BF16)
         y = dot(perm_t, y).astype(BF16)
         qg_s[:, KVW * g : KVW * (g + 1)] = dot(ident, y, NT).astype(BF16)
-    pl.when(odd)(backs[0].start)
     fetch_x.wait()
+    swap_x.wait_recv()
 
     @pl.when(odd)
     def _():
         swaps[3].wait_recv()
         kt[...] = dot(perm, kx[...], NT)
 
-    width = x_ref.shape[1]
-    for i in range(width // HALFW):
-        cols = slice(HALFW * i, HALFW * (i + 1))
-        xt[cols, :] = dot(eye(HALFW), x_ref[:, cols], NT).astype(BF16)
+    width = xx.shape[2]
+    wide = 2 * wrow
+    r = lax.broadcasted_iota(jnp.int32, (wrow, wide), 0)
+    c = lax.broadcasted_iota(jnp.int32, (wrow, wide), 1)
+    pick = (c == r + core * wrow).astype(F32).astype(BF16)
+    for part in range(2):
+        j = (me + part) % 2
+        for i in range(chips):
+            xt[wrow * i : wrow * (i + 1), t * part : t * (part + 1)] = dot(
+                pick, xx[j, :, wide * i : wide * (i + 1)], NT
+            ).astype(BF16)
 
     whole = []
     for c in range(CHUNKS):
@@ -416,57 +447,51 @@
         axis=0,
     ).astype(BF16)
     y = dot(perm_t, y).astype(BF16)
-    pg = jnp.concatenate(
-        [dot(ident, y, NT).astype(BF16), whole[0].astype(BF16), whole[2].astype(BF16)], axis=1
-    )
-
-    def to_partner():
-        return pltpu.make_async_remote_copy(
-            src_ref=wp.at[1 - core], dst_ref=pbuf, send_sem=p_send, recv_sem=p_recv,
-            device_id={"dp": dme + 1 - 2 * core}, device_id_type=MESH,
-        )
+    pgb[:t, :KVW] = dot(ident, y, NT).astype(BF16)
+    pgb[:t, KVW : KVW + HALFW] = whole[0].astype(BF16)
+    pgb[:t, KVW + HALFW :] = whole[2].astype(BF16)
+    swap_pg.start()
 
     def to_chip(k):
         return pltpu.make_async_remote_copy(
-            src_ref=asend.at[k], dst_ref=arecv.at[k], send_sem=a_send, recv_sem=a_recv.at[k],
+            src_ref=asend.at[(chip + k) % chips], dst_ref=arecv.at[k], send_sem=a_send, recv_sem=a_recv.at[k],
             device_id={"dp": ((chip + k) % chips) * 2 + core}, device_id_type=MESH,
         )
 
-    per_dot = min(8, nd)
-    for i in range(nd // per_dot):
-        part = dot(xt[wrow * per_dot * i : wrow * per_dot * (i + 1)], pg).astype(BF16)
-        for j in range(per_dot):
-            o = per_dot * i + j
-            wp[o % 2, o // 2] = part[wrow * j : wrow * (j + 1)]
-    to_partner().start()
-
-    to_partner().wait_recv()
-
-    def send_chip(k, _):
-        o = (chip + k) % chips
-        asend[k] = (wp[core, o].astype(F32) + pbuf[o].astype(F32)).astype(BF16)
-        to_chip(k).start()
-        return 0
-
-    lax.fori_loop(1, chips, send_chip, 0)
     wait_bytes(w_all.at[pl.ds(0, wrow * (nd - 1))], w_recv)
+    pg = pgb[:t]
     for i in range(width // KVW):
         rows = slice(KVW * i, KVW * (i + 1))
         ig_s[:, rows] = dot(pg, w_all[rows, :], NT).astype(BF16)
-    pl.when(odd)(backs[1].start)
+    swap_pg.wait_recv()
+    per_dot = min(4, chips)
+    for i in range(chips // per_dot):
+        part = dot(xt[wrow * per_dot * i : wrow * per_dot * (i + 1)], pgb[...]).astype(BF16)
+        for j in range(per_dot):
+            asend[per_dot * i + j] = part[wrow * j : wrow * (j + 1)]
+
+    def send_chip(k, _):
+        to_chip(k).start()
+        return 0
+
+    lax.fori_loop(1, chips, send_chip, 0)
 
     @pl.when(even)
     def _():
         qg_ref[...] = qg_s[...]
         ig_ref[...] = ig_s[...]
 
-
     def take_chip(k, total):
         to_chip(k).wait_recv()
         return total + arecv[k].astype(F32)
 
-    mine = wp[core, chip].astype(F32) + pbuf[chip].astype(F32)
-    mine = lax.fori_loop(1, chips, take_chip, mine).astype(BF16)
+    mine = lax.fori_loop(1, chips, take_chip, asend[chip].astype(F32)).astype(BF16)
+
+    @pl.when(odd)
+    def _():
+        for copy in backs:
+            copy.start()
+
 
     zrow = zsend.shape[1]
     ncol = 2 * KVW // HALFW
@@ -515,7 +540,8 @@
     wait_bytes(w_all.at[pl.ds(0, wrow * (nd - 1))], w_send)
     wait_bytes(sbuf.at[0], r_send)
     wait_bytes(sbuf.at[1, pl.ds(0, h - 1)], r_send)
-    to_partner().wait_send()
+    swap_x.wait_send()
+    swap_pg.wait_send()
     wait_bytes(asend.at[pl.ds(0, chips - 1)], a_send)
     wait_bytes(zsend.at[pl.ds(0, n - 1)], z_send)
     wait_bytes(zall.at[pl.ds(0, n - 1)], y_send)
@@ -570,10 +596,14 @@
             pltpu.VMEM((t, GROUPS * PER * DIM), BF16),
             pltpu.VMEM((n, zrow, HALFW), BF16),
         ),
-        in_specs=[vmem] * 6 + [anywhere] * 4,
+        in_specs=[anywhere] * 2 + [vmem] * 2 + [anywhere] * 6,
         out_specs=(vmem,) * 3,
         scratch_shapes=[
-            pltpu.VMEM((t, width), BF16),
+            pltpu.VMEM((t, KVW), BF16),
+            pltpu.VMEM((t, KVW), BF16),
+            pltpu.VMEM((wrow, KVW), BF16),
+            pltpu.VMEM((wrow, KVW), BF16),
+            pltpu.VMEM((2, t, width), BF16),
             pltpu.VMEM((t, GROUPS * PER * DIM), BF16),
             pltpu.VMEM((t, GROUPS * PER * DIM), BF16),
             pltpu.VMEM((t, KVW), BF16),
@@ -595,19 +625,19 @@
             pltpu.VMEM((1, q_all), F32),
             pltpu.VMEM((GROUPS, KVW, t), F32),
             pltpu.VMEM((KVW, t), F32),
-            pltpu.VMEM((width, t), BF16),
+            pltpu.VMEM((chips * wrow, 2 * t), BF16),
             pltpu.VMEM((KVW, PER * t), F32),
             pltpu.VMEM((2, CHUNKS, 2 * t, HALFW), F32),
             pltpu.VMEM((2, h, CHUNKS, t, HALFW), BF16),
             pltpu.VMEM((2, h, CHUNKS, t, HALFW), BF16),
-            pltpu.VMEM((2, chips, wrow, 2 * KVW), BF16),
-            pltpu.VMEM((chips, wrow, 2 * KVW), BF16),
+            pltpu.VMEM((2 * t, 2 * KVW), BF16),
             pltpu.VMEM((chips, wrow, 2 * KVW), BF16),
             pltpu.VMEM((chips, wrow, 2 * KVW), BF16),
             pltpu.VMEM((n, zrow, HALFW), BF16),
             pltpu.VMEM((n, zrow, HALFW), BF16),
-            dma((5,)),
+            dma((4,)),
             dma((7,)),
+            dma((8,)),
             dma((2,)),
             dma,
             dma,
@@ -617,13 +647,12 @@
             dma,
             dma((2, h, CHUNKS, SUBS)),
             dma,
-            dma,
-            dma,
             dma((chips,)),
             dma,
             dma,
             dma,
             dma,
+            pltpu.SemaphoreType.REGULAR,
         ],
         compiler_params=pltpu.CompilerParams(
             collective_id=0, has_side_effects=True, vmem_limit_bytes=61_000_000

time: 113 us -> 108 us (0.956)
  Pallas kernels: 110 us -> 106 us
    pallas_call x1, Pallas kernels: 109 us -> 105 us  [on_device(): pl.pallas_call(functools.partial(kernel, n, nd), out_shape=(pltpu.VMEM((t...]
where the time goes in v5:
time: 108 us; the launch traced here: 106 us
  Pallas kernels  106 us (98%)
    pallas_call x1, Pallas kernels, on_device(): pl.pallas_call(functools.partial(kernel, n, nd), out_shape=(pltpu.VMEM((t...  105 us

profile of v5, /device:TPU:1, one launch (start us, length us, event | category | flops | bytes accessed | tf_op | source)
XLA Modules:
  0.0 106.2 jit_solution(3988169196795522059)
XLA Ops:
  0.6 104.6 %shard_map.129 = (bf16[128,2048]{1,0:T(8,128)(2,1)S(1)}, bf16[128,1024]{1,0:T(8,128)(2,1)S(1)}, bf16[16,16,128]{2,1,0:T(8,128)(2,1)S(1)}) custom-call(bf16[128,256]{1,0:T(8,128)(2,1)} %bitcast.12, bf16[128,256]{1,0:T(8,128)(2,1)} %bitcast.13, f32[1,64]{1,0:T(1,128)} %bitcast.14, f32[1,64]{1,0:T(1,128)} %bitcast.15, bf16[64,256]{1,0:T(8,128)(2,1)} %km_hbm.1, ...), custom_call_target="tpu_custom_call" | custom-call | tf_op jit(solution)/shard_map/pallas_call | solution.py:592
  105.2 0.9 shard_map.130

commit v6 on v5

--- a/solution.py
+++ b/solution.py
@@ -81,14 +81,19 @@
     return jnp.concatenate([r * (ua - qa * f), r * (ub - qb * f)], axis=0)
 
 
+def plane_of(chips):
+    xs = 4 if chips == 16 else 2
+    return xs, chips // xs
+
+
 def kernel(
     n, nd,
     k_hbm, v_hbm, qgain_ref, kgain_ref, km_hbm, vm_hbm, x_hbm, q_hbm, do_hbm, tab_ref,
     ig_ref, qg_ref, zall,
     k_ref, v_ref, km_ref, vm_ref, xx, q_ref, do_ref, kx, own, ig_s, qg_s,
     cs, kvb, w_all, qbd, qbdt, obd, obdt, e_ref, dp_ref, mj, mrun, lsum, dsum, qt, kt, xt, dqt, acc,
-    sbuf, rbuf, pgb, asend, arecv, zsend, zrecv,
-    first_sem, in_sem, swap_send, back_recv, tab_sem, g_send, g_recv, w_send, w_recv, r_send, r_recv, a_send, a_recv,
+    sbuf, rbuf, x_row, x_col, pg_row, pg_col, a_sum, b_sum, a_in, b_in, zsend, zrecv,
+    first_sem, in_sem, swap_send, back_recv, tab_sem, g_send, g_recv, w_send, w_recv, r_send, r_recv, x_send, x_recv, p_send, row_recv, col_recv, s_send, s_recv,
     z_send, z_recv, y_send, y_recv, plane,
 ):
     t = q_ref.shape[0]
@@ -124,14 +129,13 @@
         copy.start()
     fetch_q = pltpu.make_async_copy(q_hbm, q_ref, in_sem.at[0])
     fetch_do = pltpu.make_async_copy(do_hbm, do_ref, in_sem.at[1])
-    fetch_x = pltpu.make_async_copy(x_hbm, xx.at[0], in_sem.at[2])
+    fetch_x = pltpu.make_async_copy(x_hbm, xx, in_sem.at[2])
 
     @pl.when(even)
     def _():
         fetch_q.start()
         fetch_do.start()
-
-    fetch_x.start()
+        fetch_x.start()
 
     def to_mate(i, src, dst, recv_sem):
         return pltpu.make_async_remote_copy(
@@ -145,14 +149,12 @@
         to_mate(1, q_hbm, q_ref, in_sem.at[0]),
         to_mate(2, do_hbm, do_ref, in_sem.at[1]),
         to_mate(3, k_ref, kx, in_sem.at[4]),
+        to_mate(4, x_hbm, xx, in_sem.at[2]),
     ]
-    swap_x = to_mate(4, x_hbm, xx.at[1], in_sem.at[5])
-    swap_pg = to_mate(7, pgb.at[pl.ds(0, t)], pgb.at[pl.ds(t, t)], in_sem.at[6])
     backs = [to_mate(5, qg_s, qg_ref, back_recv.at[0]), to_mate(6, ig_s, ig_ref, back_recv.at[1])]
     barrier = pltpu.get_barrier_semaphore()
 
-    xs = 4 if chips == 16 else 2
-    ys = chips // xs
+    xs, ys = plane_of(chips)
     row, col = chip // xs, chip % xs
     beside = [(row * xs + (col + i) % xs) * 2 for i in range(1, xs)]
     above = [((row + i) % ys * xs + col) * 2 for i in range(1, ys)]
@@ -235,8 +237,6 @@
         for copy in swaps:
             copy.start()
 
-    swap_x.start()
-
 
     def start_w(k, _):
         to_plane(k).start()
@@ -296,11 +296,41 @@
         if h > 2 or c >= PARTS // 2:
             to_left(2, c).start()
 
+    def in_row(j, e):
+        return (row * xs + (col + j) % xs) * 2 + (core + e) % 2
+
+    def in_col(j, e):
+        return ((row + j) % ys * xs + col) * 2 + (core + e) % 2
+
+    def to_dp(src, dst, send_sem, recv_sem, where):
+        return pltpu.make_async_remote_copy(
+            src_ref=src, dst_ref=dst, send_sem=send_sem, recv_sem=recv_sem,
+            device_id={"dp": where}, device_id_type=MESH,
+        )
+
+    row_inputs = [
+        to_dp(xt.at[:, (col + j) % xs, (core + e) % 2], x_row.at[2 * j + e], x_send.at[0], x_recv.at[0], in_row(j, e))
+        for j in range(xs) for e in range(2) if j + e
+    ]
+    col_inputs = [
+        to_dp(xt.at[(row + j) % ys, :, (core + e) % 2], x_col.at[2 * j + e], x_send.at[1], x_recv.at[1], in_col(j, e))
+        for j in range(ys) for e in range(2) if j + e
+    ]
+
     def gather_step(s, _):
         @pl.when(s == min(3, h))
         def _():
+            fetch_x.wait()
+            for i in range(chips):
+                two = dot(eye(2 * wrow), xx[:, 2 * wrow * i : 2 * wrow * (i + 1)], NT).astype(BF16)
+                xt[i // xs, i % xs, 0] = two[:wrow]
+                xt[i // xs, i % xs, 1] = two[wrow:]
             pl.semaphore_wait(plane, 2 * len(beside))
             lax.fori_loop(1, nd, start_w, 0)
+            x_row[0] = xt[:, col, core]
+            x_col[0] = xt[row, :, core]
+            for copy in row_inputs + col_inputs:
+                copy.start()
 
         for c in range(PARTS):
             def receive(copy, s=s, c=c):
@@ -410,35 +440,31 @@
         ).astype(BF16)
         y = dot(perm_t, y).astype(BF16)
         qg_s[:, KVW * g : KVW * (g + 1)] = dot(ident, y, NT).astype(BF16)
-    fetch_x.wait()
-    swap_x.wait_recv()
 
     @pl.when(odd)
     def _():
         swaps[3].wait_recv()
         kt[...] = dot(perm, kx[...], NT)
 
-    width = xx.shape[2]
-    wide = 2 * wrow
-    r = lax.broadcasted_iota(jnp.int32, (wrow, wide), 0)
-    c = lax.broadcasted_iota(jnp.int32, (wrow, wide), 1)
-    pick = (c == r + core * wrow).astype(F32).astype(BF16)
-    for part in range(2):
-        j = (me + part) % 2
-        for i in range(chips):
-            xt[wrow * i : wrow * (i + 1), t * part : t * (part + 1)] = dot(
-                pick, xx[j, :, wide * i : wide * (i + 1)], NT
-            ).astype(BF16)
-
-    whole = []
-    for c in range(CHUNKS):
+    def to_row(src, dst, where):
+        return to_dp(pg_row.at[src], pg_row.at[dst], p_send.at[0], row_recv.at[dst], where)
+
+    def to_col(src, dst, where):
+        return to_dp(pg_col.at[src], pg_col.at[dst], p_send.at[1], col_recv.at[dst], where)
+
+    def arrived(c):
         for b in range(SUBS):
             for d in range(2):
                 pass_on(d, h - 1, c, b).wait_recv()
-        whole.append(
-            acc[1 - last, c, :t] + rbuf[0, h - 1, c].astype(F32) + rbuf[1, h - 1, c].astype(F32)
-        )
-    dkt = jnp.transpose(jnp.concatenate([whole[1], whole[3]], axis=1))
+        return acc[1 - last, c, :t] + rbuf[0, h - 1, c].astype(F32) + rbuf[1, h - 1, c].astype(F32)
+
+    pg_col[0, :, :HALFW] = arrived(0).astype(BF16)
+    low = arrived(1)
+    pg_col[0, :, HALFW:] = arrived(2).astype(BF16)
+    for j in range(1, ys):
+        to_col(0, 2 * j, in_col(j, 0)).start()
+    to_col(0, 1, mate).start()
+    dkt = jnp.transpose(jnp.concatenate([low, arrived(3)], axis=1))
     y = jnp.concatenate(
         [
             rope_bwd(dkt[DIM * g : DIM * (g + 1)], kt[DIM * g : DIM * (g + 1)], cos, sin, kgain)
@@ -447,51 +473,83 @@
         axis=0,
     ).astype(BF16)
     y = dot(perm_t, y).astype(BF16)
-    pgb[:t, :KVW] = dot(ident, y, NT).astype(BF16)
-    pgb[:t, KVW : KVW + HALFW] = whole[0].astype(BF16)
-    pgb[:t, KVW + HALFW :] = whole[2].astype(BF16)
-    swap_pg.start()
-
-    def to_chip(k):
-        return pltpu.make_async_remote_copy(
-            src_ref=asend.at[(chip + k) % chips], dst_ref=arecv.at[k], send_sem=a_send, recv_sem=a_recv.at[k],
-            device_id={"dp": ((chip + k) % chips) * 2 + core}, device_id_type=MESH,
-        )
-
+    pg_row[0] = dot(ident, y, NT).astype(BF16)
+    for j in range(1, xs):
+        to_row(0, 2 * j, in_row(j, 0)).start()
+    to_row(0, 1, mate).start()
+
+    width = xx.shape[1]
     wait_bytes(w_all.at[pl.ds(0, wrow * (nd - 1))], w_recv)
-    pg = pgb[:t]
+    pg = jnp.concatenate([pg_row[0], pg_col[0]], axis=1)
     for i in range(width // KVW):
         rows = slice(KVW * i, KVW * (i + 1))
         ig_s[:, rows] = dot(pg, w_all[rows, :], NT).astype(BF16)
-    swap_pg.wait_recv()
-    per_dot = min(4, chips)
-    for i in range(chips // per_dot):
-        part = dot(xt[wrow * per_dot * i : wrow * per_dot * (i + 1)], pgb[...]).astype(BF16)
-        for j in range(per_dot):
-            asend[per_dot * i + j] = part[wrow * j : wrow * (j + 1)]
-
-    def send_chip(k, _):
-        to_chip(k).start()
-        return 0
-
-    lax.fori_loop(1, chips, send_chip, 0)
 
     @pl.when(even)
     def _():
         qg_ref[...] = qg_s[...]
         ig_ref[...] = ig_s[...]
 
-    def take_chip(k, total):
-        to_chip(k).wait_recv()
-        return total + arecv[k].astype(F32)
-
-    mine = lax.fori_loop(1, chips, take_chip, asend[chip].astype(F32)).astype(BF16)
+    wait_bytes(x_row.at[pl.ds(1, 2 * xs - 1)], x_recv.at[0])
+    wait_bytes(x_col.at[pl.ds(1, 2 * ys - 1)], x_recv.at[1])
+
+    def row_term(i):
+        return dot(x_row[i].reshape(ys * wrow, t), pg_row[i])
+
+    def col_term(i):
+        return dot(x_col[i].reshape(xs * wrow, t), pg_col[i])
+
+    to_col(0, 1, mate).wait_recv()
+    to_row(0, 1, mate).wait_recv()
+    total_row = row_term(0) + row_term(1)
+    total_col = col_term(0) + col_term(1)
+    for j in range(1, max(xs, ys)):
+        if j < ys:
+            to_col(0, 2 * j, mate).wait_recv()
+            to_col(2 * j, 2 * j + 1, mate).start()
+        if j < xs:
+            to_row(0, 2 * j, mate).wait_recv()
+            to_row(2 * j, 2 * j + 1, mate).start()
+    for j in range(1, ys):
+        total_col += col_term(2 * j)
+    for j in range(1, xs):
+        total_row += row_term(2 * j)
+    for j in range(1, ys):
+        to_col(2 * j, 2 * j + 1, mate).wait_recv()
+        total_col += col_term(2 * j + 1)
+    for i in range(xs):
+        b_sum[i] = total_col[wrow * i : wrow * (i + 1)].astype(BF16)
+    for j in range(1, xs):
+        to_row(2 * j, 2 * j + 1, mate).wait_recv()
+        total_row += row_term(2 * j + 1)
+    for i in range(ys):
+        a_sum[i] = total_row[wrow * i : wrow * (i + 1)].astype(BF16)
+
+    b_sums = [
+        to_dp(b_sum.at[(col + j) % xs], b_in.at[j], s_send.at[1], s_recv.at[1], in_row(j, 0)) for j in range(1, xs)
+    ]
+    a_sums = [
+        to_dp(a_sum.at[(row + j) % ys], a_in.at[j], s_send.at[0], s_recv.at[0], in_col(j, 0)) for j in range(1, ys)
+    ]
+    for copy in b_sums + a_sums:
+        copy.start()
 
     @pl.when(odd)
     def _():
         for copy in backs:
             copy.start()
 
+    of_keys = a_sum[row].astype(F32)
+    of_values = b_sum[col].astype(F32)
+    if xs > 1:
+        wait_bytes(b_in.at[pl.ds(1, xs - 1)], s_recv.at[1])
+    for j in range(1, xs):
+        of_values += b_in[j].astype(F32)
+    if ys > 1:
+        wait_bytes(a_in.at[pl.ds(1, ys - 1)], s_recv.at[0])
+    for j in range(1, ys):
+        of_keys += a_in[j].astype(F32)
+    mine = jnp.concatenate([of_keys, of_values], axis=1).astype(BF16)
 
     zrow = zsend.shape[1]
     ncol = 2 * KVW // HALFW
@@ -540,9 +598,14 @@
     wait_bytes(w_all.at[pl.ds(0, wrow * (nd - 1))], w_send)
     wait_bytes(sbuf.at[0], r_send)
     wait_bytes(sbuf.at[1, pl.ds(0, h - 1)], r_send)
-    swap_x.wait_send()
-    swap_pg.wait_send()
-    wait_bytes(asend.at[pl.ds(0, chips - 1)], a_send)
+    wait_bytes(x_row.at[pl.ds(1, 2 * xs - 1)], x_send.at[0])
+    wait_bytes(x_col.at[pl.ds(1, 2 * ys - 1)], x_send.at[1])
+    wait_bytes(pg_row.at[pl.ds(1, 2 * xs - 1)], p_send.at[0])
+    wait_bytes(pg_col.at[pl.ds(1, 2 * ys - 1)], p_send.at[1])
+    if xs > 1:
+        wait_bytes(b_in.at[pl.ds(1, xs - 1)], s_send.at[1])
+    if ys > 1:
+        wait_bytes(a_in.at[pl.ds(1, ys - 1)], s_send.at[0])
     wait_bytes(zsend.at[pl.ds(0, n - 1)], z_send)
     wait_bytes(zall.at[pl.ds(0, n - 1)], y_send)
 
@@ -584,6 +647,7 @@
     q_all = GROUPS * PER * t
     h = n // 2
     chips = nd // 2
+    xs, ys = plane_of(chips)
     zrow = wrow * 2 * KVW // HALFW // n
     dma = pltpu.SemaphoreType.DMA
     vmem = pl.BlockSpec(memory_space=pltpu.VMEM)
@@ -603,7 +667,7 @@
             pltpu.VMEM((t, KVW), BF16),
             pltpu.VMEM((wrow, KVW), BF16),
             pltpu.VMEM((wrow, KVW), BF16),
-            pltpu.VMEM((2, t, width), BF16),
+            pltpu.VMEM((t, width), BF16),
             pltpu.VMEM((t, GROUPS * PER * DIM), BF16),
             pltpu.VMEM((t, GROUPS * PER * DIM), BF16),
             pltpu.VMEM((t, KVW), BF16),
@@ -625,19 +689,24 @@
             pltpu.VMEM((1, q_all), F32),
             pltpu.VMEM((GROUPS, KVW, t), F32),
             pltpu.VMEM((KVW, t), F32),
-            pltpu.VMEM((chips * wrow, 2 * t), BF16),
+            pltpu.VMEM((ys, xs, 2, wrow, t), BF16),
             pltpu.VMEM((KVW, PER * t), F32),
             pltpu.VMEM((2, CHUNKS, 2 * t, HALFW), F32),
             pltpu.VMEM((2, h, CHUNKS, t, HALFW), BF16),
             pltpu.VMEM((2, h, CHUNKS, t, HALFW), BF16),
-            pltpu.VMEM((2 * t, 2 * KVW), BF16),
-            pltpu.VMEM((chips, wrow, 2 * KVW), BF16),
-            pltpu.VMEM((chips, wrow, 2 * KVW), BF16),
+            pltpu.VMEM((2 * xs, ys, wrow, t), BF16),
+            pltpu.VMEM((2 * ys, xs, wrow, t), BF16),
+            pltpu.VMEM((2 * xs, t, KVW), BF16),
+            pltpu.VMEM((2 * ys, t, KVW), BF16),
+            pltpu.VMEM((ys, wrow, KVW), BF16),
+            pltpu.VMEM((xs, wrow, KVW), BF16),
+            pltpu.VMEM((ys, wrow, KVW), BF16),
+            pltpu.VMEM((xs, wrow, KVW), BF16),
             pltpu.VMEM((n, zrow, HALFW), BF16),
             pltpu.VMEM((n, zrow, HALFW), BF16),
             dma((4,)),
+            dma((5,)),
             dma((7,)),
-            dma((8,)),
             dma((2,)),
             dma,
             dma,
@@ -646,8 +715,13 @@
             dma,
             dma,
             dma((2, h, CHUNKS, SUBS)),
-            dma,
-            dma((chips,)),
+            dma((2,)),
+            dma((2,)),
+            dma((2,)),
+            dma((2 * xs,)),
+            dma((2 * ys,)),
+            dma((2,)),
+            dma((2,)),
             dma,
             dma,
             dma,

time: 108 us -> 101 us (0.935)
  Pallas kernels: 106 us -> 99.3 us
    pallas_call x1, Pallas kernels: 105 us -> 98.4 us  [on_device(): pl.pallas_call(functools.partial(kernel, n, nd), out_shape=(pltpu.VMEM((t...]
where the time goes in v6:
time: 101 us; the launch traced here: 100 us
  Pallas kernels  99.3 us (98%)
    pallas_call x1, Pallas kernels, on_device(): pl.pallas_call(functools.partial(kernel, n, nd), out_shape=(pltpu.VMEM((t...  98.4 us

profile of v6, /device:TPU:1, one launch (start us, length us, event | category | flops | bytes accessed | tf_op | source)
XLA Modules:
  0.0 100.0 jit_solution(12996820701259422173)
XLA Ops:
  0.6 98.4 %shard_map.129 = (bf16[128,2048]{1,0:T(8,128)(2,1)S(1)}, bf16[128,1024]{1,0:T(8,128)(2,1)S(1)}, bf16[16,16,128]{2,1,0:T(8,128)(2,1)S(1)}) custom-call(bf16[128,256]{1,0:T(8,128)(2,1)} %bitcast.12, bf16[128,256]{1,0:T(8,128)(2,1)} %bitcast.13, f32[1,64]{1,0:T(1,128)} %bitcast.14, f32[1,64]{1,0:T(1,128)} %bitcast.15, bf16[64,256]{1,0:T(8,128)(2,1)} %km_hbm.1, ...), custom_call_target="tpu_custom_call" | custom-call | tf_op jit(solution)/shard_map/pallas_call | solution.py:656
  99.0 0.9 shard_map.130

commit v7 on v6

--- a/solution.py
+++ b/solution.py
@@ -209,6 +209,14 @@
             device_id={"sp": left, "dp": mate}, device_id_type=MESH,
         )
 
+    def skip(c, d):
+        part = pl.ds(c * crow, crow)
+        return pltpu.make_async_remote_copy(
+            src_ref=kvb.at[n + 2 - h if d else h - 2, part], dst_ref=kvb.at[h, part],
+            send_sem=g_send, recv_sem=g_recv.at[d, h - 1, c],
+            device_id={"sp": (me + (n - 2 if d else 2)) % n, "dp": dme}, device_id_type=MESH,
+        )
+
     def first_hop(c, d):
         part = pl.ds(c * crow, crow)
         return pltpu.make_async_remote_copy(
@@ -339,13 +347,13 @@
             def forward(copy, s=s, c=c):
                 copy(s + 1, c).start()
 
-            for copy, whole in ((to_right, c < PARTS // 2), (to_left, c >= PARTS // 2)):
-                if whole:
+            for d, copy in enumerate((to_right, to_left)):
+                if d == c // (PARTS // 2):
                     receive(copy)
-                    pl.when(s < h)(functools.partial(forward, copy))
+                    pl.when(s == h - 2)(skip(c, d).start)
                 else:
                     pl.when(s < h)(functools.partial(receive, copy))
-                    pl.when(s < h - 1)(functools.partial(forward, copy))
+                pl.when(s < h - 1)(functools.partial(forward, copy))
             first_pass((s - 1, n + 1 - s), s - 1, c)
         return 0
 
@@ -386,41 +394,48 @@
             device_id={"sp": left if d else right, "dp": mate}, device_id_type=MESH,
         )
 
-    for c in range(CHUNKS):
-        rbuf[c % 2, 0, c] = jnp.zeros((t, HALFW), BF16)
+    def far_on(d, c):
+        return pltpu.make_async_remote_copy(
+            src_ref=sbuf.at[d, 0, c], dst_ref=rbuf.at[d, 0, c],
+            send_sem=r_send, recv_sem=r_recv.at[d, 0, c, 0],
+            device_id={"sp": (me + (n - 2 if d else 2)) % n, "dp": dme}, device_id_type=MESH,
+        )
+
+    for g in range(GROUPS):
+        second_pass((h + 1, h - 1), h - 1, g, 1)
+        if g % 2 == 1:
+            for c in (g - 1, g):
+                for d in range(2):
+                    sbuf[d, 1, c] = acc[1, c, t * d : t * (d + 1)].astype(BF16)
+                    pass_on(d, 1, c, 0).start()
     for g in range(GROUPS):
         second_pass((h,), h, g, 0)
         if g % 2 == 1:
             for c in (g - 1, g):
                 d = 1 - c % 2
                 sbuf[d, 0, c] = acc[0, c, :t].astype(BF16)
-                for b in range(SUBS):
-                    pass_on(d, 0, c, b).start()
+                far_on(d, c).start()
     for g in range(GROUPS):
-        second_pass((h + 1, h - 1), h - 1, g, 1)
-
-    def add_and_send(u, c, place):
-        for b in range(SUBS):
-            for d in range(2):
-                def arrived(d=d, b=b):
-                    pass_on(d, u - 1, c, b).wait_recv()
-
-                if d == 1 - c % 2:
-                    arrived()
-                else:
-                    pl.when(u > 1)(arrived)
-                part = slice(srow * b, srow * (b + 1))
-                own = acc[place, c, t * d + srow * b : t * d + srow * (b + 1)]
-                sbuf[d, u, c, part] = (own + rbuf[d, u - 1, c, part].astype(F32)).astype(BF16)
-                pass_on(d, u, c, b).start()
-
-    def reduce_step(u, _):
+        second_pass((h + 2, h - 2), h - 2, g, 0)
+
+    def add_and_send(u, c, place, far=False):
+        for d in range(2):
+            pass_on(d, u - 1, c, 0).wait_recv()
+            total = acc[place, c, t * d : t * (d + 1)] + rbuf[d, u - 1, c].astype(F32)
+            if far and d == 1 - c % 2:
+                far_on(d, c).wait_recv()
+                total += rbuf[d, 0, c].astype(F32)
+            sbuf[d, u, c] = total.astype(BF16)
+            pass_on(d, u, c, 0).start()
+
+    def reduce_step(u, _, far=False):
         for c in range(CHUNKS):
-            add_and_send(u, c, u % 2)
+            add_and_send(u, c, u % 2, far)
             second_pass((h + 1 + u, h - 1 - u), h - 1 - u, c, (u + 1) % 2)
         return 0
 
-    lax.fori_loop(1, h - 1, reduce_step, 0)
+    reduce_step(2, 0, True)
+    lax.fori_loop(3, h - 1, reduce_step, 0)
     last = (h - 1) % 2
     for c in range(CHUNKS):
         add_and_send(h - 1, c, last)

time: 101 us -> 103 us (1.020)
  Pallas kernels: 99.3 us -> 102 us
    pallas_call x1, Pallas kernels: 98.4 us -> 101 us  [on_device(): pl.pallas_call(functools.partial(kernel, n, nd), out_shape=(pltpu.VMEM((t...]
where the time goes in v7:
time: 103 us
  Pallas kernels  102 us (99%)
    pallas_call x1, Pallas kernels, on_device(): pl.pallas_call(functools.partial(kernel, n, nd), out_shape=(pltpu.VMEM((t...  101 us

profile of v7, /device:TPU:1, one launch (start us, length us, event | category | flops | bytes accessed | tf_op | source)
XLA Modules:
  0.0 102.6 jit_solution(1188755556398902062)
XLA Ops:
  0.6 101.0 %shard_map.129 = (bf16[128,2048]{1,0:T(8,128)(2,1)S(1)}, bf16[128,1024]{1,0:T(8,128)(2,1)S(1)}, bf16[16,16,128]{2,1,0:T(8,128)(2,1)S(1)}) custom-call(bf16[128,256]{1,0:T(8,128)(2,1)} %bitcast.12, bf16[128,256]{1,0:T(8,128)(2,1)} %bitcast.13, f32[1,64]{1,0:T(1,128)} %bitcast.14, f32[1,64]{1,0:T(1,128)} %bitcast.15, bf16[64,256]{1,0:T(8,128)(2,1)} %km_hbm.1, ...), custom_call_target="tpu_custom_call" | custom-call | tf_op jit(solution)/shard_map/pallas_call | solution.py:671
  101.7 0.9 shard_map.130
